TPU v7x, 256 devices: a whole 4x4x8 slice. The times are simulated.
256 devices in a mesh: sp: 64 (over z, y, core), tp: 4 (over x).
Axes of the slice: x: 4, y: 4, z: 8, core: 2. Of those that a mesh axis runs over, the one named last changes fastest.
Arguments:
- tokens: bfloat16 [16384, 4096], P(('sp', 'tp')), may hold values from -6 to 6
- norm_gain: float32 [4096], replicated, may hold values from 0.1 to 1.9
- w_query: bfloat16 [4096, 1024], P(None, 'tp'), may hold values from -0.25 to 0.25
- w_key: bfloat16 [4096, 512], P(None, 'tp'), may hold values from -0.09375 to 0.09375
- w_value: bfloat16 [4096, 512], P(None, 'tp'), may hold values from -0.09375 to 0.09375
- score_shift: float32 [8], P('tp'), may hold values from -15 to -8
- w_conv_b: bfloat16 [4096, 1024], P(None, 'tp'), may hold values from -0.09375 to 0.09375
- w_conv_c: bfloat16 [4096, 1024], P(None, 'tp'), may hold values from -0.09375 to 0.09375
- w_conv_u: bfloat16 [4096, 1024], P(None, 'tp'), may hold values from -0.09375 to 0.09375
- conv_kernel: float32 [3, 1024], P(None, 'tp'), may hold values from -3.5 to 3.5
- w_out_att: bfloat16 [4096, 1024], P('sp', 'tp'), may hold values from -0.75 to 0.75
- w_out_conv: bfloat16 [4096, 1024], P('sp', 'tp'), may hold values from -0.1875 to 0.1875
Outputs:
- mixed: bfloat16 [16384, 4096], P(('sp', 'tp'))
- log_weight: float32 [16384, 8], P('sp', 'tp')
All inputs are finite; a program needn't handle non-finite values.
Results may differ from a plain program's by a relative error of at most 0.017.
Values may be sent and summed in bfloat16 or wider, within the bound.
A program may use at most 128 MiB of HBM per device.

v0:
```python
import jax
import jax.numpy as jnp
from jax import lax
from jax.sharding import PartitionSpec as P

HEAD_DIM = 128
CONV_K = 3
KEY_BLOCK = 1024


def laid_out(blocks, dim):
    blocks = jnp.moveaxis(blocks, 0, dim)
    lengths = blocks.shape
    return blocks.reshape(*lengths[:dim], lengths[dim] * lengths[dim + 1], *lengths[dim + 2 :])


def copy_for_each(x, axis):
    count = lax.axis_size(axis)
    return lax.all_to_all(jnp.broadcast_to(x[None], (count, *x.shape)), axis, 0, 0, tiled=True)


def gathered_copies(x, axis, dim):
    return laid_out(copy_for_each(x, axis), dim)


def shifted(value, axis, steps):
    count = lax.axis_size(axis)
    leading, last = (max(0, -steps), min(count, count - steps))
    return lax.ppermute(value, axis, [(source, source + steps) for source in range(leading, last)])


def sent_together(arrays, axis, dim, along):
    both = jnp.concatenate(arrays, axis=along)
    out, at, finished = (lax.all_gather(both, axis, axis=dim, tiled=True), 0, [])
    for a in arrays:
        finished.append(lax.slice_in_dim(out, at, at + a.shape[along], axis=along))
        at += a.shape[along]
    return tuple(finished)


def normalize(tokens, norm_gain):
    widened = tokens.astype(jnp.float32)
    inverse = lax.rsqrt(jnp.mean(widened * widened, axis=-1, keepdims=True) + 1e-06)
    return (widened * inverse * norm_gain).astype(jnp.bfloat16)


def block_terms(grouped_q, key_block, value_block, shifts, query_pos, key_first):
    scores = jnp.einsum("qhgd,khd->qhgk", grouped_q, key_block, preferred_element_type=jnp.float32)
    scores = scores * HEAD_DIM ** (-0.5) + shifts[None, :, :, None]
    key_pos = key_first + jnp.arange(KEY_BLOCK, dtype=jnp.int32)
    causal = key_pos[None, None, None, :] < query_pos[:, None, None, None]
    soft = jnp.where(causal, jax.nn.softplus(scores), 0.0)
    after_sum = lax.cumsum(soft, axis=3, reverse=True) - soft
    relative = jnp.where(causal, jnp.exp(jax.nn.log_sigmoid(scores) - after_sum), 0.0).astype(
        jnp.bfloat16
    )
    partial_value = jnp.einsum(
        "qhgk,khd->qhgd", relative, value_block, preferred_element_type=jnp.float32
    )
    return (partial_value, jnp.sum(soft, axis=3))


def attend(grouped_q, query_pos, key_whole, value_whole, shifts):
    row_count, kv_local, grouping, head_size = grouped_q.shape
    last_block = jnp.max(query_pos) // KEY_BLOCK

    def visit(step, carry):
        accum, suffix = carry
        block_no = last_block - step
        key_first = block_no * KEY_BLOCK
        key_block = lax.dynamic_slice_in_dim(key_whole, key_first, KEY_BLOCK, 0).reshape(
            KEY_BLOCK, kv_local, head_size
        )
        value_block = lax.dynamic_slice_in_dim(value_whole, key_first, KEY_BLOCK, 0).reshape(
            KEY_BLOCK, kv_local, head_size
        )
        partial_value, total = block_terms(
            grouped_q, key_block, value_block, shifts, query_pos, key_first
        )
        accum = accum + jnp.exp(-suffix)[..., None] * partial_value
        return (accum, suffix + total)

    start = (
        jnp.zeros((row_count, kv_local, grouping, head_size), jnp.float32),
        jnp.zeros((row_count, kv_local, grouping), jnp.float32),
    )
    accum, suffix = lax.fori_loop(0, last_block + 1, visit, start)
    return (
        accum.reshape(row_count, kv_local * grouping * head_size),
        suffix.reshape(row_count, kv_local * grouping),
    )


def local(
    tokens,
    norm_gain,
    w_query,
    w_key,
    w_value,
    score_shift,
    w_conv_b,
    w_conv_c,
    w_conv_u,
    conv_kernel,
    w_out_att,
    w_out_conv,
):
    weights = (w_query, w_key, w_value, w_conv_b, w_conv_c, w_conv_u)

    def project(rows_in):
        normed = normalize(rows_in, norm_gain)
        return jnp.concatenate(
            [
                jnp.dot(normed, weight, preferred_element_type=jnp.float32).astype(jnp.bfloat16)
                for weight in weights
            ],
            axis=1,
        )

    projected = project(gathered_copies(tokens, "tp", 0))
    widths = [weight.shape[1] for weight in weights]
    edges = [0]
    for width in widths:
        edges.append(edges[-1] + width)
    queries, keys, values, gate_b, gate_c, inputs_u = [
        projected[:, edges[pos] : edges[pos + 1]] for pos in range(6)
    ]
    tok_count = projected.shape[0]
    conv_local = gate_b.shape[1]
    products = (gate_c.astype(jnp.float32) * inputs_u.astype(jnp.float32)).astype(jnp.bfloat16)
    previous = shifted(products[tok_count - (CONV_K - 1) :], "sp", 1)
    key_whole, value_whole, att_rows, conv_rows = (
        *sent_together((keys, values), "sp", 0, 1),
        *sent_together((w_out_att, w_out_conv), "sp", 0, 1),
    )
    local_heads = queries.shape[1] // HEAD_DIM
    kv_local = keys.shape[1] // HEAD_DIM
    grouping = local_heads // kv_local
    shifts = score_shift.reshape(kv_local, grouping)
    sp_index = lax.axis_index("sp")
    grouped_q = queries.reshape(tok_count, kv_local, grouping, HEAD_DIM)
    query_pos = sp_index * tok_count + jnp.arange(tok_count, dtype=jnp.int32)
    attended_f, sums_all = attend(grouped_q, query_pos, key_whole, value_whole, shifts)
    attended = attended_f.astype(jnp.bfloat16)
    log_weight = jnp.log(jnp.maximum(-jnp.expm1(-sums_all), 0.05))
    extended = jnp.concatenate([previous, products], axis=0)
    summed = jnp.zeros((tok_count, conv_local), jnp.float32)
    for tap in range(CONV_K):
        summed = summed + conv_kernel[tap][None, :] * extended[tap : tap + tok_count].astype(
            jnp.float32
        )
    convolved = (gate_b.astype(jnp.float32) * summed).astype(jnp.bfloat16)
    contract = (((1,), (1,)), ((), ()))
    share = lax.dot_general(attended, att_rows, contract, preferred_element_type=jnp.float32)
    share = share + lax.dot_general(
        convolved, conv_rows, contract, preferred_element_type=jnp.float32
    )
    rounded = share.astype(jnp.bfloat16).astype(jnp.float32)
    mixed = lax.psum_scatter(rounded.astype(jnp.bfloat16), "tp", scatter_dimension=0, tiled=True)
    return (mixed, log_weight)


def solution(mesh):
    return jax.shard_map(
        local,
        mesh=mesh,
        in_specs=(
            P(("sp", "tp"), None),
            P(),
            P(None, "tp"),
            P(None, "tp"),
            P(None, "tp"),
            P("tp"),
            P(None, "tp"),
            P(None, "tp"),
            P(None, "tp"),
            P(None, "tp"),
            P("sp", "tp"),
            P("sp", "tp"),
        ),
        out_specs=(P(("sp", "tp"), None), P("sp", "tp")),
        check_vma=False,
    )
```

profile of v0, /device:TPU:248, one launch (start us, length us, event | category | flops | bytes accessed | tf_op | source)
XLA Modules:
  0.0 476.3 jit_solution(7275596186314889997)
XLA Ops:
  8.6 30.4 %all_to_all.5 = bf16[4,64,4096]{2,1,0:T(8,128)(2,1)S(1)} all-to-all(bf16[4,64,4096]{2,1,0:T(8,128)(2,1)S(1)} %broadcast_in_dim.33), channel_id=1, replica_groups=mesh['sp'=64,'tp'=4] {'tp'}, dimensions={0} | all-to-all | bytes 4194304 | tf_op jit(solution)/shard_map/all_to_all | solution.py:19
  60.5 70.2 %all-gather.3.cloned.1.call-done = bf16[16384,256]{0,1:T(8,128)(2,1)} async-done(((bf16[256,256]{0,1:T(8,128)(2,1)}), bf16[16384,256]{0,1:T(8,128)(2,1)}) %all-gather.3.cloned.1.call-update) | async-done | bytes 8388624 | tf_op jit(solution)/shard_map/all_gather | solution.py:34
  130.7 5.8 %fusion.56 = (bf16[16384,128]{0,1:T(8,128)(2,1)}, bf16[16384,128]{0,1:T(8,128)(2,1)}) fusion(bf16[16384,256]{0,1:T(8,128)(2,1)} %all-gather.3.cloned.1.call-done), kind=kLoop, calls=%fused_computation.86 | loop fusion | bytes 16777216 | tf_op jit(solution)/shard_map/slice | solution.py:36
  136.6 290.1 %while.13 = (s32[]{:T(128)}, f32[256,1,2,128]{0,3,2,1:T(8,128)S(1)}, f32[256,1,2]{0,2,1:T(2,128)S(1)}, s32[]{:T(128)}, s32[]{:T(128)}, /*index=5*/bf16[16384,128...) while((s32[]{:T(128)}, ...), condition=%wide.region_6.7_spmd.clone, body=%wide.region_2.6_spmd.clone.sunk | while | flops 352224512 | bytes 50340156 | solution.py:87
  137.0 3.8 fusion.81
  140.9 5.0 %fusion.82 = f32[256,1,2,8,128]{0,3,2,1,4:T(8,128)S(1)} fusion(f32[256,1,2,8,128]{0,4,3,2,1:T(8,128)S(1)} %bitcast.137), kind=kOutput, calls=%fused_computation.19.clone.1 | output fusion | flops 66584576 | bytes 4194304 | tf_op jit(solution)/shard_map/reduce-window
  155.2 3.8 fusion.81
  159.0 5.0 %fusion.82 = f32[256,1,2,8,128]{0,3,2,1,4:T(8,128)S(1)} fusion(f32[256,1,2,8,128]{0,4,3,2,1:T(8,128)S(1)} %bitcast.137), kind=kOutput, calls=%fused_computation.19.clone.1 | output fusion | flops 66584576 | bytes 4194304 | tf_op jit(solution)/shard_map/reduce-window
  177.1 5.0 %fusion.82 = f32[256,1,2,8,128]{0,3,2,1,4:T(8,128)S(1)} fusion(f32[256,1,2,8,128]{0,4,3,2,1:T(8,128)S(1)} %bitcast.137), kind=kOutput, calls=%fused_computation.19.clone.1 | output fusion | flops 66584576 | bytes 4194304 | tf_op jit(solution)/shard_map/reduce-window
  191.5 3.8 fusion.81
  195.3 5.0 %fusion.82 = f32[256,1,2,8,128]{0,3,2,1,4:T(8,128)S(1)} fusion(f32[256,1,2,8,128]{0,4,3,2,1:T(8,128)S(1)} %bitcast.137), kind=kOutput, calls=%fused_computation.19.clone.1 | output fusion | flops 66584576 | bytes 4194304 | tf_op jit(solution)/shard_map/reduce-window
  209.6 3.8 fusion.81
  213.4 5.0 %fusion.82 = f32[256,1,2,8,128]{0,3,2,1,4:T(8,128)S(1)} fusion(f32[256,1,2,8,128]{0,4,3,2,1:T(8,128)S(1)} %bitcast.137), kind=kOutput, calls=%fused_computation.19.clone.1 | output fusion | flops 66584576 | bytes 4194304 | tf_op jit(solution)/shard_map/reduce-window
  227.7 3.8 fusion.81
  231.6 5.0 %fusion.82 = f32[256,1,2,8,128]{0,3,2,1,4:T(8,128)S(1)} fusion(f32[256,1,2,8,128]{0,4,3,2,1:T(8,128)S(1)} %bitcast.137), kind=kOutput, calls=%fused_computation.19.clone.1 | output fusion | flops 66584576 | bytes 4194304 | tf_op jit(solution)/shard_map/reduce-window
  245.8 3.8 fusion.81
  249.7 5.0 %fusion.82 = f32[256,1,2,8,128]{0,3,2,1,4:T(8,128)S(1)} fusion(f32[256,1,2,8,128]{0,4,3,2,1:T(8,128)S(1)} %bitcast.137), kind=kOutput, calls=%fused_computation.19.clone.1 | output fusion | flops 66584576 | bytes 4194304 | tf_op jit(solution)/shard_map/reduce-window
  263.9 3.8 fusion.81
  267.8 5.0 %fusion.82 = f32[256,1,2,8,128]{0,3,2,1,4:T(8,128)S(1)} fusion(f32[256,1,2,8,128]{0,4,3,2,1:T(8,128)S(1)} %bitcast.137), kind=kOutput, calls=%fused_computation.19.clone.1 | output fusion | flops 66584576 | bytes 4194304 | tf_op jit(solution)/shard_map/reduce-window
  285.9 5.0 %fusion.82 = f32[256,1,2,8,128]{0,3,2,1,4:T(8,128)S(1)} fusion(f32[256,1,2,8,128]{0,4,3,2,1:T(8,128)S(1)} %bitcast.137), kind=kOutput, calls=%fused_computation.19.clone.1 | output fusion | flops 66584576 | bytes 4194304 | tf_op jit(solution)/shard_map/reduce-window
  300.2 3.8 fusion.81
  304.0 5.0 %fusion.82 = f32[256,1,2,8,128]{0,3,2,1,4:T(8,128)S(1)} fusion(f32[256,1,2,8,128]{0,4,3,2,1:T(8,128)S(1)} %bitcast.137), kind=kOutput, calls=%fused_computation.19.clone.1 | output fusion | flops 66584576 | bytes 4194304 | tf_op jit(solution)/shard_map/reduce-window
  318.3 3.8 fusion.81
  322.1 5.0 %fusion.82 = f32[256,1,2,8,128]{0,3,2,1,4:T(8,128)S(1)} fusion(f32[256,1,2,8,128]{0,4,3,2,1:T(8,128)S(1)} %bitcast.137), kind=kOutput, calls=%fused_computation.19.clone.1 | output fusion | flops 66584576 | bytes 4194304 | tf_op jit(solution)/shard_map/reduce-window
  340.2 5.0 %fusion.82 = f32[256,1,2,8,128]{0,3,2,1,4:T(8,128)S(1)} fusion(f32[256,1,2,8,128]{0,4,3,2,1:T(8,128)S(1)} %bitcast.137), kind=kOutput, calls=%fused_computation.19.clone.1 | output fusion | flops 66584576 | bytes 4194304 | tf_op jit(solution)/shard_map/reduce-window
  358.4 5.0 %fusion.82 = f32[256,1,2,8,128]{0,3,2,1,4:T(8,128)S(1)} fusion(f32[256,1,2,8,128]{0,4,3,2,1:T(8,128)S(1)} %bitcast.137), kind=kOutput, calls=%fused_computation.19.clone.1 | output fusion | flops 66584576 | bytes 4194304 | tf_op jit(solution)/shard_map/reduce-window
  376.5 5.0 %fusion.82 = f32[256,1,2,8,128]{0,3,2,1,4:T(8,128)S(1)} fusion(f32[256,1,2,8,128]{0,4,3,2,1:T(8,128)S(1)} %bitcast.137), kind=kOutput, calls=%fused_computation.19.clone.1 | output fusion | flops 66584576 | bytes 4194304 | tf_op jit(solution)/shard_map/reduce-window
  394.6 5.0 %fusion.82 = f32[256,1,2,8,128]{0,3,2,1,4:T(8,128)S(1)} fusion(f32[256,1,2,8,128]{0,4,3,2,1:T(8,128)S(1)} %bitcast.137), kind=kOutput, calls=%fused_computation.19.clone.1 | output fusion | flops 66584576 | bytes 4194304 | tf_op jit(solution)/shard_map/reduce-window
  412.7 5.0 %fusion.82 = f32[256,1,2,8,128]{0,3,2,1,4:T(8,128)S(1)} fusion(f32[256,1,2,8,128]{0,4,3,2,1:T(8,128)S(1)} %bitcast.137), kind=kOutput, calls=%fused_computation.19.clone.1 | output fusion | flops 66584576 | bytes 4194304 | tf_op jit(solution)/shard_map/reduce-window
  426.8 4.3 fusion.32
  431.1 7.1 %fusion.28 = bf16[256,4096]{1,0:T(8,128)(2,1)} fusion(f32[256,4096]{1,0:T(8,128)} %fusion.32, bf16[4096,512]{1,0:T(8,128)(2,1)} %all-gather.5.cloned.1.call-done, bf16[256,4096]{1,0:T(8,128)(2,1)} %copy-done.3, bf16[4096,256]{1,0:T(8,128)(2,1)S(1)} %copy-done, bf16[256,256]{1,0:T(8,128)(2,1)S(1)} %fusion.36, bf16[2,256]{1,0:T(2,128)(2,1)S(1)} %collective-permute-done, ...), kind=kOutput, calls=%fused_computation.43 | convolution fusion | flops 1077018624 | bytes 12718080 | tf_op jit(solution)/shard_map/dot_general | solution.py:155
  438.9 31.0 %reduce-scatter.2.cloned.1.call-done = bf16[64,4096]{1,0:T(8,128)(2,1)} async-done(((bf16[256,4096]{1,0:T(8,128)(2,1)}), bf16[64,4096]{1,0:T(8,128)(2,1)}) %reduce-scatter.2.cloned.1.call-update) | async-done | bytes 524304 | tf_op jit(solution)/shard_map/reduce_scatter | solution.py:159
  (332 shorter events, 193.9 us)
Async XLA Ops:
  7.2 423.9 %copy-start = (bf16[4096,256]{1,0:T(8,128)(2,1)S(1)}, bf16[4096,256]{1,0:T(8,128)(2,1)}, u32[]{:S(2)}) copy-start(bf16[4096,256]{1,0:T(8,128)(2,1)} %param.20) | copy-start | bytes 6291460
  7.2 123.5 %all-gather.3.cloned.1.call-start = ((), (), s32[]{:S(2)}) async-start(), calls=%async_computation.2 | async-start | bytes 8519680 | tf_op jit(solution)/shard_map/all_gather | solution.py:34
  41.1 2.3 copy-start.8
  43.4 2.9 copy-start.3
  43.5 2.0 copy-start.9
  45.4 1.6 copy-start.10
  45.4 1.6 copy-start.11
  45.4 5.6 %copy-start.14 = (f32[3,256]{1,0:T(4,128)S(1)}, f32[3,256]{1,0:T(4,128)}, u32[]{:S(2)}) copy-start(f32[3,256]{1,0:T(4,128)} %param.23) | copy-start | bytes 9220
  47.0 379.8 %all-gather.5.cloned.1.call-start = ((), (), s32[]{:S(2)}) async-start(), calls=%async_computation.3 | async-start | bytes 4259840 | tf_op jit(solution)/shard_map/all_gather | solution.py:34
  47.8 422.1 %reduce-scatter.2.cloned.1.call-start = ((), (), s32[]{:S(2)}) async-start(), calls=%async_computation.4 | async-start | bytes 2621440 | tf_op jit(solution)/shard_map/reduce_scatter | solution.py:159
  54.3 3.1 copy-start.4
  54.3 3.5 copy-start.7
  58.6 78.0 %copy-start.13 = (f32[2]{0:T(128)S(1)}, f32[2]{0:T(128)}, u32[]{:S(2)}) copy-start(f32[2]{0:T(128)} %param.19) | copy-start | bytes 28
  58.6 372.5 %collective-permute-start = (bf16[2,256]{1,0:T(2,128)(2,1)S(1)}, bf16[2,256]{1,0:T(2,128)(2,1)S(1)}, u32[]{:S(2)}, u32[]{:S(2)}) collective-permute-start(bf16[2,256]{1,0:T(2,128)(2,1)S(1)} %slice.53), channel_id=1, source_target_pairs={{0,4},{4,8},{8,12},{12,16},{16,20},{20,24},{24,28},{28,32},{32,36}... | collective-permute-start | bytes 3080 | tf_op jit(solution)/shard_map/ppermute | solution.py:29
  147.3 1.6 copy-start.2
  148.9 1.6 copy-start.5
  165.4 1.6 copy-start.2
  167.0 1.6 copy-start.5
  183.5 1.6 copy-start.2
  185.1 1.6 copy-start.5
  219.8 1.6 copy-start.2
  221.4 1.6 copy-start.5
  274.2 1.6 copy-start.2
  275.8 1.6 copy-start.5
  292.3 1.6 copy-start.2
  293.9 1.6 copy-start.5
  310.4 1.6 copy-start.2
  312.0 1.6 copy-start.5
  346.6 1.6 copy-start.2
  364.8 1.6 copy-start.2
  366.3 1.6 copy-start.5
  382.9 1.6 copy-start.2
  (32 other events, 45.3 us)
Sparse Core Ops, SparseCore 0:
  47.1 83.5 all-gather.2
  133.5 76.2 all-gather.4
  438.4 31.3 reduce-scatter.1
where the time goes:
time: 482 us; the launch traced here: 476 us
  other arithmetic  140 us (29%)
  matrix products  102 us (21%)
  waiting for transfers between devices  101 us (21%)
  local copies, waits for them, and re-layouts  82.1 us (17%)
  blocking collectives  30.4 us (6%)
  between operations  16.5 us (3%)
    another operation x32, other arithmetic  81.3 us
    all_gather x2, waiting for transfers between devices, sent_together(): lax.all_gather(both, axis, axis=dim, tiled=True)  70.2 us
    dot_general x16, matrix products, block_terms(): jnp.einsum('qhgd,khd->qhgk', grouped_q, key_block, preferred_element_type...  61.4 us
    convert_element_type x16, other arithmetic, block_terms(): jnp.where(causal, jnp.exp(jax.nn.log_sigmoid(scores) - after_sum), 0.0)  50 us
    while x96, local copies, waits for them, and re-layouts  49.4 us
    reduce_scatter x1, waiting for transfers between devices, local(): lax.psum_scatter(rounded.astype(jnp.bfloat16), 'tp', scatter_dimension=0,...  31 us
    all_to_all x1, blocking collectives, copy_for_each(): lax.all_to_all(jnp.broadcast_to(x[None], (count, *x.shape)), axis, 0, 0,...  30.4 us
    another operation x64, local copies, waits for them, and re-layouts  22.1 us
  transfers between devices with their start and end apart: 4, of which 2 were waited for; matrix products, arithmetic and copies ran while one was open for 54% of the time, Pallas kernels for 0%

commit v1 on v0

--- a/solution.py
+++ b/solution.py
@@ -1,11 +1,12 @@
 import jax
 import jax.numpy as jnp
 from jax import lax
+from jax.experimental import pallas as pl
+from jax.experimental.pallas import tpu as pltpu
 from jax.sharding import PartitionSpec as P
 
 HEAD_DIM = 128
 CONV_K = 3
-KEY_BLOCK = 1024
 
 
 def laid_out(blocks, dim):
@@ -44,51 +45,123 @@
     return (widened * inverse * norm_gain).astype(jnp.bfloat16)
 
 
-def block_terms(grouped_q, key_block, value_block, shifts, query_pos, key_first):
-    scores = jnp.einsum("qhgd,khd->qhgk", grouped_q, key_block, preferred_element_type=jnp.float32)
-    scores = scores * HEAD_DIM ** (-0.5) + shifts[None, :, :, None]
-    key_pos = key_first + jnp.arange(KEY_BLOCK, dtype=jnp.int32)
-    causal = key_pos[None, None, None, :] < query_pos[:, None, None, None]
-    soft = jnp.where(causal, jax.nn.softplus(scores), 0.0)
-    after_sum = lax.cumsum(soft, axis=3, reverse=True) - soft
-    relative = jnp.where(causal, jnp.exp(jax.nn.log_sigmoid(scores) - after_sum), 0.0).astype(
-        jnp.bfloat16
-    )
-    partial_value = jnp.einsum(
-        "qhgk,khd->qhgd", relative, value_block, preferred_element_type=jnp.float32
-    )
-    return (partial_value, jnp.sum(soft, axis=3))
-
-
-def attend(grouped_q, query_pos, key_whole, value_whole, shifts):
-    row_count, kv_local, grouping, head_size = grouped_q.shape
-    last_block = jnp.max(query_pos) // KEY_BLOCK
-
-    def visit(step, carry):
-        accum, suffix = carry
-        block_no = last_block - step
-        key_first = block_no * KEY_BLOCK
-        key_block = lax.dynamic_slice_in_dim(key_whole, key_first, KEY_BLOCK, 0).reshape(
-            KEY_BLOCK, kv_local, head_size
-        )
-        value_block = lax.dynamic_slice_in_dim(value_whole, key_first, KEY_BLOCK, 0).reshape(
-            KEY_BLOCK, kv_local, head_size
-        )
-        partial_value, total = block_terms(
-            grouped_q, key_block, value_block, shifts, query_pos, key_first
-        )
-        accum = accum + jnp.exp(-suffix)[..., None] * partial_value
-        return (accum, suffix + total)
-
-    start = (
-        jnp.zeros((row_count, kv_local, grouping, head_size), jnp.float32),
-        jnp.zeros((row_count, kv_local, grouping), jnp.float32),
-    )
-    accum, suffix = lax.fori_loop(0, last_block + 1, visit, start)
-    return (
-        accum.reshape(row_count, kv_local * grouping * head_size),
-        suffix.reshape(row_count, kv_local * grouping),
-    )
+F32 = jnp.float32
+BF16 = jnp.bfloat16
+TILE = 256
+NT = (((1,), (1,)), ((), ()))
+
+
+def softplus(z):
+    small = jnp.exp(-jnp.abs(z))
+    whole = 1.0 + small
+    return jnp.maximum(z, 0.0) + (jnp.log(whole) + (small - (whole - 1.0)))
+
+
+def attention_kernel(
+    q_ref, k_ref, v_ref, shift_ref, later_ref, out_ref, sum_ref, q_split, acc, carry, score, base, after
+):
+    last = lax.axis_index("sp")
+    heads = [pl.ds(0, TILE), pl.ds(TILE, TILE)]
+    for h in range(2):
+        scaled = q_ref[:, h * HEAD_DIM : (h + 1) * HEAD_DIM].astype(F32) * HEAD_DIM ** (-0.5)
+        high = scaled.astype(BF16)
+        q_split[heads[h], 0:HEAD_DIM] = high
+        q_split[heads[h], HEAD_DIM : 2 * HEAD_DIM] = (scaled - high.astype(F32)).astype(BF16)
+    acc[...] = jnp.zeros_like(acc)
+    carry[...] = jnp.zeros_like(carry)
+
+    def rows_of(tile):
+        return pl.ds(pl.multiple_of(jnp.maximum(tile, 0) * TILE, TILE), TILE)
+
+    def scores(tile, slot):
+        key = k_ref[rows_of(tile), :]
+        twice = jnp.concatenate([key, key], axis=1)
+        for h in range(2):
+            score[slot, heads[h], :] = (
+                lax.dot_general(q_split[heads[h], :], twice, NT, preferred_element_type=F32)
+                + shift_ref[h]
+            )
+
+    def sums(slot, masked=False):
+        for h in range(2):
+            z = score[slot, heads[h], :]
+            soft = softplus(z)
+            if masked:
+                row = lax.broadcasted_iota(jnp.int32, (TILE, TILE), 0)
+                col = lax.broadcasted_iota(jnp.int32, (TILE, TILE), 1)
+                soft = jnp.where(col < row, soft, 0.0)
+                z = jnp.where(col < row, z, -jnp.inf)
+            held = carry[heads[h], :]
+            base[slot, heads[h], :] = (z - soft) - jnp.concatenate([held, held], axis=1)
+            after[slot, heads[h], :] = jnp.dot(
+                soft.astype(BF16), later_ref[...], preferred_element_type=F32
+            )
+            carry[heads[h], :] = held + jnp.sum(soft, axis=1, keepdims=True)
+
+    def weigh(tile, slot):
+        value = v_ref[rows_of(tile), :]
+        for h in range(2):
+            weight = jnp.exp(base[slot, heads[h], :] - after[slot, heads[h], :])
+            acc[heads[h], :] += jnp.dot(weight.astype(BF16), value, preferred_element_type=F32)
+
+    scores(last, 0)
+    sums(0, True)
+    scores(last - 1, 1)
+
+    def two_tiles(step, _):
+        tile = last - 1 - 2 * step
+        scores(tile - 1, 0)
+        sums(1)
+        weigh(tile + 1, 0)
+        scores(tile - 2, 1)
+        sums(0)
+        weigh(tile, 1)
+        return 0
+
+    lax.fori_loop(0, last // 2, two_tiles, 0)
+
+    @pl.when(last % 2 == 1)
+    def _():
+        sums(1)
+        weigh(1, 0)
+        weigh(0, 1)
+
+    @pl.when(last % 2 == 0)
+    def _():
+        weigh(0, 0)
+
+    for h in range(2):
+        out_ref[:, h * HEAD_DIM : (h + 1) * HEAD_DIM] = acc[heads[h], :].astype(BF16)
+        sum_ref[:, h * HEAD_DIM : (h + 1) * HEAD_DIM] = carry[heads[h], :]
+
+
+def attend(queries, key_whole, value_whole, score_shift):
+    row_count, width = queries.shape
+    later = (jnp.arange(TILE)[:, None] > jnp.arange(TILE)[None, :]).astype(BF16)
+    vmem = pl.BlockSpec(memory_space=pltpu.VMEM)
+    attended, sums = pl.pallas_call(
+        attention_kernel,
+        name="attention",
+        out_shape=(
+            jax.ShapeDtypeStruct((row_count, width), BF16),
+            jax.ShapeDtypeStruct((row_count, width), F32),
+        ),
+        in_specs=[vmem, vmem, vmem, pl.BlockSpec(memory_space=pltpu.SMEM), vmem],
+        out_specs=(vmem, vmem),
+        scratch_shapes=[
+            pltpu.VMEM((2 * TILE, 2 * HEAD_DIM), BF16),
+            pltpu.VMEM((2 * TILE, HEAD_DIM), F32),
+            pltpu.VMEM((2 * TILE, HEAD_DIM), F32),
+            pltpu.VMEM((2, 2 * TILE, TILE), F32),
+            pltpu.VMEM((2, 2 * TILE, TILE), F32),
+            pltpu.VMEM((2, 2 * TILE, TILE), F32),
+        ],
+        compiler_params=pltpu.CompilerParams(vmem_limit_bytes=40 * 1024 * 1024),
+        cost_estimate=pl.CostEstimate(
+            flops=12 * 10**9, bytes_accessed=9 * 10**6, transcendentals=25 * 10**6
+        ),
+    )(queries, key_whole, value_whole, score_shift, later)
+    return attended, sums[:, ::HEAD_DIM]
 
 
 def local(
@@ -133,15 +206,7 @@
         *sent_together((keys, values), "sp", 0, 1),
         *sent_together((w_out_att, w_out_conv), "sp", 0, 1),
     )
-    local_heads = queries.shape[1] // HEAD_DIM
-    kv_local = keys.shape[1] // HEAD_DIM
-    grouping = local_heads // kv_local
-    shifts = score_shift.reshape(kv_local, grouping)
-    sp_index = lax.axis_index("sp")
-    grouped_q = queries.reshape(tok_count, kv_local, grouping, HEAD_DIM)
-    query_pos = sp_index * tok_count + jnp.arange(tok_count, dtype=jnp.int32)
-    attended_f, sums_all = attend(grouped_q, query_pos, key_whole, value_whole, shifts)
-    attended = attended_f.astype(jnp.bfloat16)
+    attended, sums_all = attend(queries, key_whole, value_whole, score_shift)
     log_weight = jnp.log(jnp.maximum(-jnp.expm1(-sums_all), 0.05))
     extended = jnp.concatenate([previous, products], axis=0)
     summed = jnp.zeros((tok_count, conv_local), jnp.float32)

time: 482 us -> 258 us (0.54)
  other arithmetic: 140 us -> 4.21 us
  matrix products: 102 us -> 17.4 us
  local copies, waits for them, and re-layouts: 82.1 us -> 9.34 us
  waiting for transfers between devices: 101 us -> 145 us
  Pallas kernels: 0 us -> 32.3 us
    dot_general x32 -> x0, matrix products: 81.8 us -> none  [the longest x16 61.4 us: block_terms(): jnp.einsum('qhgd,khd->qhgk', grouped_q, key_block, preferred_element_type...]
    another operation x32 -> x0, other arithmetic: 81.3 us -> none
    convert_element_type x17 -> x1, other arithmetic: 50 us -> 0.02 us  [attend(): later = (jnp.arange(TILE)[:, None] > jnp.arange(TILE)[None, :]).astype(BF16)]
    while x96 -> x0, local copies, waits for them, and re-layouts: 49.4 us -> none
    all_gather x2, waiting for transfers between devices: 70.2 us -> 113 us  [sent_together(): lax.all_gather(both, axis, axis=dim, tiled=True)]
    pallas_call x0 -> x1, Pallas kernels: none -> 32.3 us  [attend(): pl.pallas_call(attention_kernel, name='attention', out_shape=(jax.ShapeDt...]
    another operation x64 -> x0, local copies, waits for them, and re-layouts: 22.1 us -> none
  transfers between devices with their start and end apart: 4 -> 4, of which waited for: 2 -> 3; matrix products, arithmetic and copies ran while one was open for 54% -> 6% of each run, Pallas kernels for 0% -> 13%
where the time goes in v1:
time: 258 us; the launch traced here: 255 us
  waiting for transfers between devices  145 us (56%)
  Pallas kernels  32.3 us (13%)
  blocking collectives  30.4 us (12%)
  matrix products  17.4 us (7%)
  between operations  14 us (5%)
  local copies, waits for them, and re-layouts  9.34 us (4%)
  other arithmetic  4.21 us (2%)
    all_gather x2, waiting for transfers between devices, sent_together(): lax.all_gather(both, axis, axis=dim, tiled=True)  113 us
    pallas_call x1, Pallas kernels, attend(): pl.pallas_call(attention_kernel, name='attention', out_shape=(jax.ShapeDt...  32.3 us
    reduce_scatter x1, waiting for transfers between devices, local(): lax.psum_scatter(rounded.astype(jnp.bfloat16), 'tp', scatter_dimension=0,...  31.7 us
    all_to_all x1, blocking collectives, copy_for_each(): lax.all_to_all(jnp.broadcast_to(x[None], (count, *x.shape)), axis, 0, 0,...  30.4 us
    dot_general x1, matrix products, local(): lax.dot_general(convolved, conv_rows, contract, preferred_element_type=jn...  7.18 us
    dot_general x5, matrix products, project(): jnp.dot(normed, weight, preferred_element_type=jnp.float32)  5.9 us
  transfers between devices with their start and end apart: 4, of which 3 were waited for; matrix products, arithmetic and copies ran while one was open for 6% of the time, Pallas kernels for 13%

profile of v1, /device:TPU:248, one launch (start us, length us, event | category | flops | bytes accessed | tf_op | source)
XLA Modules:
  0.0 254.5 jit_solution(15488394112439822384)
XLA Ops:
  7.2 0.0 all-gather.3.cloned.1.call-start
  7.2 1.4 broadcast_in_dim.2
  8.6 30.4 %all_to_all.5 = bf16[4,64,4096]{2,1,0:T(8,128)(2,1)S(1)} all-to-all(bf16[4,64,4096]{2,1,0:T(8,128)(2,1)S(1)} %broadcast_in_dim.2), channel_id=1, replica_groups=mesh['sp'=64,'tp'=4] {'tp'}, dimensions={0} | all-to-all | bytes 4194304 | tf_op jit(solution)/shard_map/all_to_all | solution.py:20
  39.1 1.3 copy-done.4
  40.4 0.5 multiply_reduce_fusion
  40.9 0.1 rsqrt.12
  41.0 0.1 copy-done.10
  41.1 2.3 fusion.2
  43.5 0.7 convolution_convert_fusion.4
  44.2 1.3 copy-done.7
  45.5 0.7 convolution_convert_fusion.5
  46.2 0.7 pad_maximum_fusion.2
  46.9 0.0 all-gather.3.cloned.1.call-update
  46.9 0.0 all-gather.5.cloned.1.call-start
  46.9 0.6 pad_maximum_fusion.3
  47.6 0.0 all-gather.5.cloned.1.call-update
  47.6 0.0 reduce-scatter.2.cloned.1.call-start
  47.7 3.1 %fusion.9 = f32[256,256]{1,0:T(8,128)S(1)} fusion(bf16[256,4096]{1,0:T(8,128)(2,1)} %copy-done.2, bf16[4096,256]{1,0:T(8,128)(2,1)} %param.19), kind=kOutput, calls=%fused_computation.14 | convolution fusion | flops 537001984 | bytes 4456448 | tf_op jit(solution)/shard_map/dot_general | solution.py:187
  50.8 0.4 copy-done.5
  51.2 0.7 fusion.8
  51.9 1.9 collective-permute-start
  53.9 0.7 convolution_convert_fusion.3.q_ref
  54.6 70.3 %all-gather.3.cloned.1.call-done = bf16[16384,256]{1,0:T(8,128)(2,1)} async-done(((bf16[256,256]{1,0:T(8,128)(2,1)}), bf16[16384,256]{1,0:T(8,128)(2,1)}) %all-gather.3.cloned.1.call-update) | async-done | bytes 8388624 | tf_op jit(solution)/shard_map/all_gather | solution.py:35
  125.0 3.8 %fusion.29 = (bf16[16384,128]{1,0:T(8,128)(2,1)S(1)}, bf16[16384,128]{1,0:T(8,128)(2,1)S(1)}) fusion(bf16[16384,256]{1,0:T(8,128)(2,1)} %all-gather.3.cloned.1.call-done), kind=kLoop, calls=%fused_computation.45 | loop fusion | bytes 16777216 | tf_op jit(solution)/shard_map/slice | solution.py:37
  128.7 32.3 %attention.1 = (bf16[256,256]{1,0:T(8,128)(2,1)S(1)}, f32[256,256]{1,0:T(8,128)S(1)}) custom-call(bf16[256,256]{1,0:T(8,128)(2,1)S(1)} %convolution_convert_fusion.3.q_ref, bf16[16384,128]{1,0:T(8,128)(2,1)S(1)} %get-tuple-element.11.k_ref, bf16[16384,128]{1,0:T(8,128)(2,1)S(1)} %get-tuple-element.10.v_ref, f32[2]{0:T(128)S(1)} %copy-done.1, ...), custom_call_target="tpu_custom_call" | custom-call | flops 12000000000 | bytes 9000000 | tf_op jit(solution)/shard_map/attention/pallas_call | solution.py:142
  161.0 42.8 %all-gather.5.cloned.1.call-done = bf16[4096,512]{1,0:T(8,128)(2,1)} async-done(((bf16[64,512]{1,0:T(8,128)(2,1)}), bf16[4096,512]{1,0:T(8,128)(2,1)}) %all-gather.5.cloned.1.call-update) | async-done | bytes 4194320 | tf_op jit(solution)/shard_map/all_gather | solution.py:35
  203.8 4.3 %fusion.4 = f32[256,4096]{1,0:T(8,128)} fusion(bf16[256,256]{1,0:T(8,128)(2,1)S(1)} %get-tuple-element.4, bf16[4096,512]{1,0:T(8,128)(2,1)} %all-gather.5.cloned.1.call-done), kind=kOutput, calls=%fused_computation.7 | convolution fusion | flops 536870912 | bytes 6422528 | tf_op jit(solution)/shard_map/dot_general | solution.py:219
  208.1 7.2 %fusion = bf16[256,4096]{1,0:T(8,128)(2,1)} fusion(f32[256,4096]{1,0:T(8,128)} %fusion.4, bf16[4096,512]{1,0:T(8,128)(2,1)} %all-gather.5.cloned.1.call-done, bf16[256,4096]{1,0:T(8,128)(2,1)} %copy-done.2, bf16[4096,256]{1,0:T(8,128)(2,1)S(1)} %copy-done, bf16[256,256]{1,0:T(8,128)(2,1)S(1)} %fusion.8, bf16[2,256]{1,0:T(2,128)(2,1)S(1)} %collective-permute-done, ...), kind=kOutput, calls=%fused_computation.1 | convolution fusion | flops 1077018624 | bytes 12718080 | tf_op jit(solution)/shard_map/dot_general | solution.py:220
  215.3 0.3 slice.43
  215.6 0.1 maximum_log_fusion
  215.6 0.7 copy.19
  216.3 31.7 %reduce-scatter.2.cloned.1.call-done = bf16[64,4096]{1,0:T(8,128)(2,1)} async-done(((bf16[256,4096]{1,0:T(8,128)(2,1)}), bf16[64,4096]{1,0:T(8,128)(2,1)}) %reduce-scatter.2.cloned.1.call-update) | async-done | bytes 524304 | tf_op jit(solution)/shard_map/reduce_scatter | solution.py:224
  (28 shorter events, 0.1 us)
Async XLA Ops:
  7.2 200.9 %copy-start = (bf16[4096,256]{1,0:T(8,128)(2,1)S(1)}, bf16[4096,256]{1,0:T(8,128)(2,1)}, u32[]{:S(2)}) copy-start(bf16[4096,256]{1,0:T(8,128)(2,1)} %param.18) | copy-start | bytes 6291460
  7.2 117.8 %all-gather.3.cloned.1.call-start = ((), (), s32[]{:S(2)}) async-start(), calls=%async_computation.2 | async-start | bytes 8519680 | tf_op jit(solution)/shard_map/all_gather | solution.py:35
  39.1 1.3 copy-start.4
  40.4 0.7 copy-start.10
  41.1 2.3 copy-start.6
  43.4 2.7 %copy-start.2 = (bf16[256,4096]{1,0:T(8,128)(2,1)}, bf16[256,4096]{1,0:T(8,128)(2,1)S(1)}, u32[]{:S(2)}) copy-start(bf16[256,4096]{1,0:T(8,128)(2,1)S(1)} %fusion.2) | copy-start | bytes 6291460
  43.5 2.0 copy-start.7
  45.4 1.5 copy-start.8
  45.4 1.5 copy-start.9
  45.4 2.3 copy-start.11
  46.9 156.9 %all-gather.5.cloned.1.call-start = ((), (), s32[]{:S(2)}) async-start(), calls=%async_computation.3 | async-start | bytes 4259840 | tf_op jit(solution)/shard_map/all_gather | solution.py:35
  47.6 200.4 %reduce-scatter.2.cloned.1.call-start = ((), (), s32[]{:S(2)}) async-start(), calls=%async_computation.4 | async-start | bytes 2621440 | tf_op jit(solution)/shard_map/reduce_scatter | solution.py:224
  47.7 3.1 %copy-start.3 = (bf16[256,4096]{1,0:T(8,128)(2,1)S(1)}, bf16[256,4096]{1,0:T(8,128)(2,1)}, u32[]{:S(2)}) copy-start(bf16[256,4096]{1,0:T(8,128)(2,1)} %copy-done.2) | copy-start | bytes 6291460
  47.7 3.5 %copy-start.5 = (bf16[4096,256]{1,0:T(8,128)(2,1)S(1)}, bf16[4096,256]{1,0:T(8,128)(2,1)}, u32[]{:S(2)}) copy-start(bf16[4096,256]{1,0:T(8,128)(2,1)} %param.20) | copy-start | bytes 6291460
  51.2 2.7 %copy-start.12 = (bf16[4096,256]{1,0:T(8,128)(2,1)S(1)}, bf16[4096,256]{1,0:T(8,128)(2,1)}, u32[]{:S(2)}) copy-start(bf16[4096,256]{1,0:T(8,128)(2,1)} %param.14) | copy-start | bytes 6291460
  51.9 156.1 %collective-permute-start = (bf16[2,256]{1,0:T(2,128)(2,1)S(1)}, bf16[2,256]{1,0:T(2,128)(2,1)S(1)}, u32[]{:S(2)}, u32[]{:S(2)}) collective-permute-start(bf16[2,256]{1,0:T(2,128)(2,1)S(1)} %slice.47), channel_id=1, source_target_pairs={{0,4},{4,8},{8,12},{12,16},{16,20},{20,24},{24,28},{28,32},{32,36}... | collective-permute-start | bytes 3080 | tf_op jit(solution)/shard_map/ppermute | solution.py:30
  54.6 74.1 %copy-start.1 = (f32[2]{0:T(128)S(1)}, f32[2]{0:T(128)}, u32[]{:S(2)}) copy-start(f32[2]{0:T(128)} %shift_ref.1) | copy-start | bytes 28
Sparse Core Ops, SparseCore 0:
  47.0 77.9 all-gather.2
  127.7 76.0 all-gather.4
  215.4 32.5 reduce-scatter.1

commit v2 on v1

--- a/solution.py
+++ b/solution.py
@@ -7,21 +7,8 @@
 
 HEAD_DIM = 128
 CONV_K = 3
-
-
-def laid_out(blocks, dim):
-    blocks = jnp.moveaxis(blocks, 0, dim)
-    lengths = blocks.shape
-    return blocks.reshape(*lengths[:dim], lengths[dim] * lengths[dim + 1], *lengths[dim + 2 :])
-
-
-def copy_for_each(x, axis):
-    count = lax.axis_size(axis)
-    return lax.all_to_all(jnp.broadcast_to(x[None], (count, *x.shape)), axis, 0, 0, tiled=True)
-
-
-def gathered_copies(x, axis, dim):
-    return laid_out(copy_for_each(x, axis), dim)
+F32 = jnp.float32
+BF16 = jnp.bfloat16
 
 
 def shifted(value, axis, steps):
@@ -30,23 +17,12 @@
     return lax.ppermute(value, axis, [(source, source + steps) for source in range(leading, last)])
 
 
-def sent_together(arrays, axis, dim, along):
-    both = jnp.concatenate(arrays, axis=along)
-    out, at, finished = (lax.all_gather(both, axis, axis=dim, tiled=True), 0, [])
-    for a in arrays:
-        finished.append(lax.slice_in_dim(out, at, at + a.shape[along], axis=along))
-        at += a.shape[along]
-    return tuple(finished)
-
-
 def normalize(tokens, norm_gain):
     widened = tokens.astype(jnp.float32)
     inverse = lax.rsqrt(jnp.mean(widened * widened, axis=-1, keepdims=True) + 1e-06)
     return (widened * inverse * norm_gain).astype(jnp.bfloat16)
 
 
-F32 = jnp.float32
-BF16 = jnp.bfloat16
 TILE = 256
 NT = (((1,), (1,)), ((), ()))
 
@@ -164,6 +140,248 @@
     return attended, sums[:, ::HEAD_DIM]
 
 
+UP, DOWN, NEXT, BACK, OTHER = range(5)
+ZS, YS, CORES = 8, 4, 2
+
+
+def plan():
+    sends = {}
+    for dz in range(-3, 5):
+        for dy in range(-1, 3):
+            first, second = [], []
+            if dy == 0:
+                if 0 <= dz < 4:
+                    first.append((UP, dz + 1, 0))
+                if -3 < dz <= 0:
+                    first.append((DOWN, dz - 1, 0))
+                first += [(NEXT, dz, 1), (BACK, dz, -1)]
+            if dy == 1 and dz % 2 == 0:
+                first.append((NEXT, dz, 2))
+            if dy == -1 and dz % 2 == 1:
+                first.append((BACK, dz, 2))
+            if dz == 0:
+                if dy == 0:
+                    second += [(NEXT, 0, 1), (BACK, 0, -1)]
+                if dy == 1:
+                    second.append((NEXT, 0, 2))
+            if 0 <= dz < 3 or (dz == 3 and dy % 2 == 0):
+                second.append((UP, dz + 1, dy))
+            if -3 < dz <= 0:
+                second.append((DOWN, dz - 1, dy))
+            if dz == -3 and dy % 2 == 1:
+                second.append((DOWN, 4, dy))
+            sends[0, dz, dy] = first
+            sends[1, dz, dy] = second
+    order = sorted(
+        (key for key in sends if key[1:] != (0, 0)),
+        key=lambda key: (abs(key[1]) + abs(key[2]), abs(key[2]) if key[0] == 0 else abs(key[1]), key),
+    )
+    return sends, order
+
+
+def chunk_of(dz, dy):
+    return (dz + 3) * YS + dy + 1
+
+
+class Gather:
+    def __init__(self, own, whole, rows, here_sem, side_sem, send_sem):
+        self.own, self.whole, self.rows = own, whole, rows
+        self.here_sem, self.side_sem, self.send_sem = here_sem, side_sem, send_sem
+        sp = lax.axis_index("sp")
+        self.z, self.y, self.core = sp // (YS * CORES), (sp // CORES) % YS, sp % CORES
+        self.sends, self.order = plan()
+
+    def sp_of(self, z, y, core):
+        return (((z + ZS) % ZS) * YS + (y + YS) % YS) * CORES + core
+
+    def neighbour(self, way):
+        z, y, core = self.z, self.y, self.core
+        return {
+            UP: self.sp_of(z + 1, y, core),
+            DOWN: self.sp_of(z - 1, y, core),
+            NEXT: self.sp_of(z, y + 1, core),
+            BACK: self.sp_of(z, y - 1, core),
+            OTHER: self.sp_of(z, y, 1 - core),
+        }[way]
+
+    def slot(self, half, dz, dy, core):
+        origin = self.sp_of(self.z - dz, self.y - dy, core)
+        return self.whole[half].at[pl.ds(pl.multiple_of(origin * self.rows, self.rows), self.rows), :]
+
+    def copy(self, half, dz, dy, way, sem):
+        dst = self.slot(half, dz, dy, self.core)
+        src = self.own[half] if (dz, dy) == (0, 0) else dst
+        return pltpu.make_async_remote_copy(
+            src_ref=src,
+            dst_ref=dst,
+            send_sem=self.send_sem.at[half],
+            recv_sem=sem,
+            device_id={"sp": self.neighbour(way)},
+            device_id_type=pl.DeviceIdType.MESH,
+        )
+
+    def pass_on(self, half, dz, dy):
+        for way, to_dz, to_dy in self.sends[half, dz, dy]:
+            self.copy(half, dz, dy, way, self.here_sem.at[half, chunk_of(to_dz % 8 - 8 * (to_dz % 8 > 4), to_dy)]).start()
+        self.copy(half, dz, dy, OTHER, self.side_sem.at[half, dz + 3]).start()
+
+    def begin(self):
+        for half, ways in ((0, (UP, DOWN)), (1, (NEXT, BACK)), (0, (NEXT, BACK)), (1, (UP, DOWN))):
+            for way, to_dz, to_dy in self.sends[half, 0, 0]:
+                if way in ways:
+                    self.copy(half, 0, 0, way, self.here_sem.at[half, chunk_of(to_dz, to_dy)]).start()
+        for half in range(2):
+            self.copy(half, 0, 0, OTHER, self.side_sem.at[half, 3]).start()
+
+    def arrive(self, key):
+        half, dz, dy = key
+        self.copy(half, dz, dy, UP, self.here_sem.at[half, chunk_of(dz, dy)]).wait_recv()
+        self.pass_on(half, dz, dy)
+
+    def side(self, half, dz):
+        plane = self.whole[half].at[pl.ds(0, YS * self.rows), :]
+        pltpu.make_async_copy(plane, plane, self.side_sem.at[half, dz + 3]).wait()
+
+    def finish(self):
+        for half in range(2):
+            sent = self.whole[half].at[pl.ds(0, (ZS * YS * CORES - 1) * self.rows), :]
+            pltpu.make_async_copy(sent, sent, self.send_sem.at[half]).wait()
+
+
+def greet(gather, around=()):
+    barrier = pltpu.get_barrier_semaphore()
+    targets = [{"sp": gather.neighbour(way)} for way in (UP, DOWN, NEXT, BACK, OTHER)] + list(around)
+    for target in targets:
+        pl.semaphore_signal(barrier, inc=1, device_id=target, device_id_type=pl.DeviceIdType.MESH)
+    pl.semaphore_wait(barrier, len(targets))
+
+
+GATHER_SEMS = (
+    pltpu.SemaphoreType.DMA((2, ZS * YS)),
+    pltpu.SemaphoreType.DMA((2, ZS)),
+    pltpu.SemaphoreType.DMA((2,)),
+)
+
+
+def keys_kernel(key_ref, value_ref, key_out, value_out, here_sem, side_sem, send_sem, own_sem):
+    gather = Gather((key_ref, value_ref), (key_out, value_out), key_ref.shape[0], here_sem, side_sem, send_sem)
+    greet(gather)
+    gather.begin()
+    kept = [
+        pltpu.make_async_copy(gather.own[half], gather.slot(half, 0, 0, gather.core), own_sem.at[half])
+        for half in range(2)
+    ]
+    for copy in kept:
+        copy.start()
+    for key in gather.order:
+        gather.arrive(key)
+    for half in range(2):
+        for dz in range(-3, 5):
+            gather.side(half, dz)
+    for copy in kept:
+        copy.wait()
+    gather.finish()
+
+
+def gathered_keys(keys, values):
+    shape = (keys.shape[0] * ZS * YS * CORES, keys.shape[1])
+    vmem = pl.BlockSpec(memory_space=pltpu.VMEM)
+    return pl.pallas_call(
+        keys_kernel,
+        name="gather_keys",
+        out_shape=(jax.ShapeDtypeStruct(shape, BF16),) * 2,
+        in_specs=[vmem] * 2,
+        out_specs=(vmem,) * 2,
+        scratch_shapes=[*GATHER_SEMS, pltpu.SemaphoreType.DMA((2,))],
+        compiler_params=pltpu.CompilerParams(
+            collective_id=1, has_side_effects=True, vmem_limit_bytes=24 * 1024 * 1024
+        ),
+    )(keys, values)
+
+
+def tokens_kernel(
+    tokens_ref, att_ref, conv_ref, rows_out, att_out, conv_out,
+    here_sem, side_sem, send_sem, own_sem, ring_sem, ring_send,
+):
+    gather = Gather((att_ref, conv_ref), (att_out, conv_out), att_ref.shape[0], here_sem, side_sem, send_sem)
+    tp, count = lax.axis_index("tp"), 4
+    right, left = {"tp": (tp + 1) % count}, {"tp": (tp + count - 1) % count}
+    greet(gather, (right, left))
+    rows = tokens_ref.shape[0]
+    part = rows // 2
+
+    def piece(origin, at):
+        return rows_out.at[pl.ds(pl.multiple_of(((origin + count) % count) * rows + at * part, part), part), :]
+
+    def ring(origin, at, target, number, mine):
+        return pltpu.make_async_remote_copy(
+            src_ref=tokens_ref.at[pl.ds(at * part, part), :] if mine else piece(origin, at),
+            dst_ref=piece(origin, at),
+            send_sem=ring_send.at[number],
+            recv_sem=ring_sem.at[number],
+            device_id=target,
+            device_id_type=pl.DeviceIdType.MESH,
+        )
+
+    sent = [ring(tp, 0, right, 0, True), ring(tp, 1, left, 2, True), ring(tp, 1, right, 1, True), ring(tp, 0, left, 3, True)]
+    for copy in sent:
+        copy.start()
+    gather.begin()
+    kept = [
+        pltpu.make_async_copy(gather.own[half], gather.slot(half, 0, 0, gather.core), own_sem.at[half])
+        for half in range(2)
+    ]
+    kept.append(
+        pltpu.make_async_copy(tokens_ref, rows_out.at[pl.ds(pl.multiple_of(tp * rows, rows), rows), :], own_sem.at[2])
+    )
+    for copy in kept:
+        copy.start()
+    for position, key in enumerate(gather.order):
+        if position == 20:
+            ring(tp - 1, 0, right, 0, False).wait_recv()
+            sent.append(ring(tp - 1, 0, right, 4, False))
+            sent[-1].start()
+            ring(tp + 1, 1, left, 2, False).wait_recv()
+            sent.append(ring(tp + 1, 1, left, 5, False))
+            sent[-1].start()
+        gather.arrive(key)
+    for number, (origin, at) in enumerate(((tp - 1, 1), (tp + 1, 0), (tp - 2, 0), (tp + 2, 1))):
+        ring(origin, at, right, (1, 3, 4, 5)[number], False).wait_recv()
+    for half in range(2):
+        for dz in range(-3, 5):
+            gather.side(half, dz)
+    for copy in kept:
+        copy.wait()
+    for copy in sent:
+        copy.wait_send()
+    gather.finish()
+
+
+def gathered_rows(tokens, w_out_att, w_out_conv):
+    vmem = pl.BlockSpec(memory_space=pltpu.VMEM)
+    many = ZS * YS * CORES
+    return pl.pallas_call(
+        tokens_kernel,
+        name="gather_rows",
+        out_shape=(
+            jax.ShapeDtypeStruct((tokens.shape[0] * 4, tokens.shape[1]), BF16),
+            jax.ShapeDtypeStruct((w_out_att.shape[0] * many, w_out_att.shape[1]), BF16),
+            jax.ShapeDtypeStruct((w_out_conv.shape[0] * many, w_out_conv.shape[1]), BF16),
+        ),
+        in_specs=[vmem] * 3,
+        out_specs=(vmem,) * 3,
+        scratch_shapes=[
+            *GATHER_SEMS,
+            pltpu.SemaphoreType.DMA((3,)),
+            pltpu.SemaphoreType.DMA((6,)),
+            pltpu.SemaphoreType.DMA((6,)),
+        ],
+        compiler_params=pltpu.CompilerParams(
+            collective_id=2, has_side_effects=True, vmem_limit_bytes=24 * 1024 * 1024
+        ),
+    )(tokens, w_out_att, w_out_conv)
+
+
 def local(
     tokens,
     norm_gain,
@@ -190,7 +408,8 @@
             axis=1,
         )
 
-    projected = project(gathered_copies(tokens, "tp", 0))
+    rows, att_rows, conv_rows = gathered_rows(tokens, w_out_att, w_out_conv)
+    projected = project(rows)
     widths = [weight.shape[1] for weight in weights]
     edges = [0]
     for width in widths:
@@ -202,10 +421,7 @@
     conv_local = gate_b.shape[1]
     products = (gate_c.astype(jnp.float32) * inputs_u.astype(jnp.float32)).astype(jnp.bfloat16)
     previous = shifted(products[tok_count - (CONV_K - 1) :], "sp", 1)
-    key_whole, value_whole, att_rows, conv_rows = (
-        *sent_together((keys, values), "sp", 0, 1),
-        *sent_together((w_out_att, w_out_conv), "sp", 0, 1),
-    )
+    key_whole, value_whole = gathered_keys(keys, values)
     attended, sums_all = attend(queries, key_whole, value_whole, score_shift)
     log_weight = jnp.log(jnp.maximum(-jnp.expm1(-sums_all), 0.05))
     extended = jnp.concatenate([previous, products], axis=0)

time: 258 us -> 164 us (0.64)
  the two profiles are of different devices: /device:TPU:248 before, /device:TPU:1 now
where the time goes in v2:
time: 164 us
  Pallas kernels  69.9 us (43%)
  waiting for transfers between devices  55.6 us (34%)
  between operations  14.2 us (9%)
  matrix products  13.5 us (8%)
  local copies, waits for them, and re-layouts  7.29 us (4%)
  starting transfers between devices  2.09 us (1%)
    reduce_scatter x1, waiting for transfers between devices, local(): lax.psum_scatter(rounded.astype(jnp.bfloat16), 'tp', scatter_dimension=0,...  55.5 us
    pallas_call x1, Pallas kernels, gathered_keys(): pl.pallas_call(keys_kernel, name='gather_keys', out_shape=(jax.ShapeDtype...  35.3 us
    pallas_call x1, Pallas kernels, gathered_rows(): pl.pallas_call(tokens_kernel, name='gather_rows', out_shape=(jax.ShapeDty...  32.6 us
    dot_general x1, matrix products, local(): lax.dot_general(convolved, conv_rows, contract, preferred_element_type=jn...  7.2 us
    unnamed x29, local copies, waits for them, and re-layouts  7.02 us
    dot_general x5, matrix products, project(): jnp.dot(normed, weight, preferred_element_type=jnp.float32)  3.55 us
  transfers between devices with their start and end apart: 2, of which 1 were waited for; matrix products, arithmetic and copies ran while one was open for 4% of the time, Pallas kernels for 23%

profile of v2, /device:TPU:1, one launch (start us, length us, event | category | flops | bytes accessed | tf_op | source)
XLA Modules:
  0.0 163.7 jit_solution(7201803028217406890)
XLA Ops:
  7.2 0.0 copy-start
  7.2 0.0 reduce-scatter.2.cloned.1.call-start
  7.2 1.2 copy-done.2
  8.4 0.8 copy-done.3
  9.2 0.8 copy-done.4
  9.9 32.6 %gather_rows.1 = (bf16[256,4096]{1,0:T(8,128)(2,1)S(1)}, bf16[4096,256]{1,0:T(8,128)(2,1)S(1)}, bf16[4096,256]{1,0:T(8,128)(2,1)S(1)}) custom-call(bf16[64,4096]{1,0:T(8,128)(2,1)S(1)} %copy-done.2, bf16[64,256]{1,0:T(8,128)(2,1)S(1)} %copy-done.3, bf16[64,256]{1,0:T(8,128)(2,1)S(1)} %copy-done.4), custom_call_target="tpu_custom_call" | custom-call | tf_op jit(solution)/shard_map/gather_rows/pallas_call | solution.py:363
  42.6 0.5 fusion.1
  43.1 0.0 copy-start.7
  43.1 0.6 fusion.3
  43.7 0.2 copy-done.1
  43.9 1.0 copy-done.7
  44.9 0.7 fusion.7
  45.6 1.6 copy-done.8
  47.2 0.7 fusion.6
  48.0 0.0 copy-start.10
  48.0 2.1 %collective-permute-start = (bf16[2,256]{1,0:T(2,128)(2,1)S(1)}, bf16[2,256]{1,0:T(2,128)(2,1)S(1)}, u32[]{:S(2)}, u32[]{:S(2)}) collective-permute-start(bf16[2,256]{1,0:T(2,128)(2,1)S(1)} %slice.28), channel_id=1, source_target_pairs={{0,4},{4,8},{8,12},{12,16},{16,20},{20,24},{24,28},{28,32},{32,36}... | collective-permute-start | bytes 3080 | tf_op jit(solution)/shard_map/ppermute | solution.py:17
  50.1 0.7 convolution_convert_fusion.4.value_ref
  50.8 0.0 copy-start.13
  50.8 0.7 convolution_convert_fusion.5.key_ref
  51.5 0.8 copy-done.13
  52.4 0.7 convolution_convert_fusion.3.q_ref
  53.1 35.3 %gather_keys.1 = (bf16[16384,128]{1,0:T(8,128)(2,1)S(1)}, bf16[16384,128]{1,0:T(8,128)(2,1)S(1)}) custom-call(bf16[256,128]{1,0:T(8,128)(2,1)S(1)} %convolution_convert_fusion.5.key_ref, bf16[256,128]{1,0:T(8,128)(2,1)S(1)} %convolution_convert_fusion.4.value_ref), custom_call_target="tpu_custom_call" | custom-call | tf_op jit(solution)/shard_map/gather_keys/pallas_call | solution.py:289
  88.4 2.0 %attention.1 = (bf16[256,256]{1,0:T(8,128)(2,1)S(1)}, f32[256,256]{1,0:T(8,128)S(1)}) custom-call(bf16[256,256]{1,0:T(8,128)(2,1)S(1)} %convolution_convert_fusion.3.q_ref, bf16[16384,128]{1,0:T(8,128)(2,1)S(1)} %get-tuple-element.10.k_ref, bf16[16384,128]{1,0:T(8,128)(2,1)S(1)} %get-tuple-element.11.v_ref, f32[2]{0:T(128)S(1)} %copy-done.5, ...), custom_call_target="tpu_custom_call" | custom-call | flops 12000000000 | bytes 9000000 | tf_op jit(solution)/shard_map/attention/pallas_call | solution.py:118
  90.4 0.0 copy-start.12
  90.4 2.7 %fusion.28 = f32[256,4096]{1,0:T(8,128)} fusion(bf16[256,256]{1,0:T(8,128)(2,1)S(1)} %get-tuple-element.12, bf16[4096,256]{1,0:T(8,128)(2,1)S(1)} %get-tuple-element.13), kind=kOutput, calls=%fused_computation.42 | convolution fusion | flops 536870912 | bytes 6422528 | tf_op jit(solution)/shard_map/dot_general | solution.py:435
  93.1 0.0 collective-permute-done
  93.1 7.2 %fusion = bf16[256,4096]{1,0:T(8,128)(2,1)} fusion(f32[256,4096]{1,0:T(8,128)} %fusion.28, bf16[4096,256]{1,0:T(8,128)(2,1)} %copy-done.1, bf16[256,4096]{1,0:T(8,128)(2,1)} %copy-done.6, bf16[4096,256]{1,0:T(8,128)(2,1)S(1)} %copy-done, bf16[256,256]{1,0:T(8,128)(2,1)S(1)} %fusion.6, bf16[2,256]{1,0:T(2,128)(2,1)S(1)} %collective-permute-done, ...), kind=kOutput, calls=%fused_computation.3 | convolution fusion | flops 1077018624 | bytes 12718080 | tf_op jit(solution)/shard_map/dot_general | solution.py:436
  100.3 0.0 reduce-scatter.2.cloned.1.call-update
  100.3 0.3 slice.27
  100.6 0.1 maximum_log_fusion
  100.7 0.7 copy.14
  101.3 55.5 %reduce-scatter.2.cloned.1.call-done = bf16[64,4096]{1,0:T(8,128)(2,1)} async-done(((bf16[256,4096]{1,0:T(8,128)(2,1)}), bf16[64,4096]{1,0:T(8,128)(2,1)}) %reduce-scatter.2.cloned.1.call-update) | async-done | bytes 524304 | tf_op jit(solution)/shard_map/reduce_scatter | solution.py:440
  (20 shorter events, 0.1 us)
Async XLA Ops:
  7.2 86.0 %copy-start = (bf16[4096,256]{1,0:T(8,128)(2,1)S(1)}, bf16[4096,256]{1,0:T(8,128)(2,1)}, u32[]{:S(2)}) copy-start(bf16[4096,256]{1,0:T(8,128)(2,1)} %param.18) | copy-start | bytes 6291460
  7.2 149.7 %reduce-scatter.2.cloned.1.call-start = ((), (), s32[]{:S(2)}) async-start(), calls=%async_computation.1 | async-start | bytes 2621440 | tf_op jit(solution)/shard_map/reduce_scatter | solution.py:440
  7.2 1.2 copy-start.2
  8.4 0.8 copy-start.3
  9.2 0.8 copy-start.4
  9.9 33.2 %copy-start.11 = (f32[4096]{0:T(1024)S(1)}, f32[4096]{0:T(1024)}, u32[]{:S(2)}) copy-start(f32[4096]{0:T(1024)} %param.13) | copy-start | bytes 49156
  42.6 1.4 copy-start.1
  43.1 1.8 %copy-start.7 = (bf16[4096,256]{1,0:T(8,128)(2,1)S(1)}, bf16[4096,256]{1,0:T(8,128)(2,1)}, u32[]{:S(2)}) copy-start(bf16[4096,256]{1,0:T(8,128)(2,1)} %param.19) | copy-start | bytes 6291460
  44.9 6.6 %copy-start.6 = (bf16[256,4096]{1,0:T(8,128)(2,1)}, bf16[256,4096]{1,0:T(8,128)(2,1)S(1)}, u32[]{:S(2)}) copy-start(bf16[256,4096]{1,0:T(8,128)(2,1)S(1)} %fusion.3) | copy-start | bytes 6291460
  44.9 2.3 %copy-start.8 = (bf16[4096,256]{1,0:T(8,128)(2,1)S(1)}, bf16[4096,256]{1,0:T(8,128)(2,1)}, u32[]{:S(2)}) copy-start(bf16[4096,256]{1,0:T(8,128)(2,1)} %param.20) | copy-start | bytes 6291460
  47.2 2.8 %copy-start.9 = (bf16[4096,128]{1,0:T(8,128)(2,1)S(1)}, bf16[4096,128]{1,0:T(8,128)(2,1)}, u32[]{:S(2)}) copy-start(bf16[4096,128]{1,0:T(8,128)(2,1)} %param.16) | copy-start | bytes 3145732
  48.0 2.8 %copy-start.10 = (bf16[4096,128]{1,0:T(8,128)(2,1)S(1)}, bf16[4096,128]{1,0:T(8,128)(2,1)}, u32[]{:S(2)}) copy-start(bf16[4096,128]{1,0:T(8,128)(2,1)} %param.15) | copy-start | bytes 3145732
  48.0 45.1 %collective-permute-start = (bf16[2,256]{1,0:T(2,128)(2,1)S(1)}, bf16[2,256]{1,0:T(2,128)(2,1)S(1)}, u32[]{:S(2)}, u32[]{:S(2)}) collective-permute-start(bf16[2,256]{1,0:T(2,128)(2,1)S(1)} %slice.28), channel_id=1, source_target_pairs={{0,4},{4,8},{8,12},{12,16},{16,20},{20,24},{24,28},{28,32},{32,36}... | collective-permute-start | bytes 3080 | tf_op jit(solution)/shard_map/ppermute | solution.py:17
  50.8 1.6 copy-start.13
  52.4 36.0 %copy-start.5 = (f32[2]{0:T(128)S(1)}, f32[2]{0:T(128)}, u32[]{:S(2)}) copy-start(f32[2]{0:T(128)} %shift_ref.1) | copy-start | bytes 28
  90.4 2.7 %copy-start.12 = (f32[3,256]{1,0:T(4,128)S(1)}, f32[3,256]{1,0:T(4,128)}, u32[]{:S(2)}) copy-start(f32[3,256]{1,0:T(4,128)} %param.21) | copy-start | bytes 9220
Sparse Core Ops, SparseCore 0:
  100.5 56.3 reduce-scatter.1

commit v3 on v2

--- a/solution.py
+++ b/solution.py
@@ -382,6 +382,103 @@
     )(tokens, w_out_att, w_out_conv)
 
 
+OUT_BLOCKS = 8
+BLOCK_ORDER = (0, 4, 1, 5, 2, 6, 3, 7)
+
+
+def output_kernel(
+    att_ref, conv_ref, att_rows, conv_rows, out_ref, share, from_left, from_right, passing, passed,
+    share_send, passed_send, left_sem, right_sem, passing_sem,
+):
+    tp, count = lax.axis_index("tp"), 4
+    right, left = (tp + 1) % count, (tp + count - 1) % count
+    across = (tp + 2) % count
+    barrier = pltpu.get_barrier_semaphore()
+    for target in (left, right):
+        pl.semaphore_signal(barrier, inc=1, device_id={"tp": target}, device_id_type=pl.DeviceIdType.MESH)
+    pl.semaphore_wait(barrier, 2)
+    rows = out_ref.shape[0]
+    width = out_ref.shape[1] // OUT_BLOCKS
+    half = OUT_BLOCKS // 2
+
+    def columns(block):
+        return pl.ds(block * width, width)
+
+    def rows_for(target):
+        return pl.ds(pl.multiple_of(target * rows, rows), rows)
+
+    def remote(src, dst, send, recv, target):
+        return pltpu.make_async_remote_copy(
+            src_ref=src, dst_ref=dst, send_sem=send, recv_sem=recv,
+            device_id={"tp": target}, device_id_type=pl.DeviceIdType.MESH,
+        )
+
+    def onward(block):
+        low = block < half
+        return remote(
+            share.at[rows_for(across), columns(block)], passing.at[:, columns(block)],
+            share_send.at[0, block], passing_sem.at[block], left if low else right,
+        )
+
+    def direct(block):
+        low = block < half
+        return remote(
+            share.at[rows_for(right if low else left), columns(block)],
+            (from_left if low else from_right).at[:, columns(block)],
+            share_send.at[1, block], (left_sem if low else right_sem).at[block], right if low else left,
+        )
+
+    def summed(block):
+        low = block < half
+        return remote(
+            passed.at[:, columns(block)], (from_right if low else from_left).at[:, columns(block)],
+            passed_send.at[block], (right_sem if low else left_sem).at[block], left if low else right,
+        )
+
+    for block in BLOCK_ORDER:
+        part = lax.dot_general(att_ref[...], att_rows[columns(block), :], NT, preferred_element_type=F32)
+        part = part + lax.dot_general(conv_ref[...], conv_rows[columns(block), :], NT, preferred_element_type=F32)
+        share[:, columns(block)] = part.astype(BF16)
+        onward(block).start()
+        direct(block).start()
+    for block in BLOCK_ORDER:
+        onward(block).wait_recv()
+        mine = share[rows_for(left if block < half else right), columns(block)]
+        passed[:, columns(block)] = (mine.astype(F32) + passing[:, columns(block)].astype(F32)).astype(BF16)
+        summed(block).start()
+    for block in BLOCK_ORDER:
+        direct(block).wait_recv()
+        summed(block).wait_recv()
+        total = share[rows_for(tp), columns(block)].astype(F32) + from_left[:, columns(block)].astype(F32)
+        out_ref[:, columns(block)] = (total + from_right[:, columns(block)].astype(F32)).astype(BF16)
+    for block in range(OUT_BLOCKS):
+        onward(block).wait_send()
+        direct(block).wait_send()
+        summed(block).wait_send()
+
+
+def mixed_rows(attended, convolved, att_rows, conv_rows):
+    count, features = attended.shape[0], att_rows.shape[0]
+    rows = count // 4
+    vmem = pl.BlockSpec(memory_space=pltpu.VMEM)
+    slab = pltpu.VMEM((rows, features), BF16)
+    sems = pltpu.SemaphoreType.DMA((OUT_BLOCKS,))
+    return pl.pallas_call(
+        output_kernel,
+        name="output",
+        out_shape=jax.ShapeDtypeStruct((rows, features), BF16),
+        in_specs=[vmem] * 4,
+        out_specs=vmem,
+        scratch_shapes=[
+            pltpu.VMEM((count, features), BF16), slab, slab, slab, slab,
+            pltpu.SemaphoreType.DMA((2, OUT_BLOCKS)), sems, sems, sems, sems,
+        ],
+        compiler_params=pltpu.CompilerParams(
+            collective_id=3, has_side_effects=True, vmem_limit_bytes=24 * 1024 * 1024
+        ),
+    )(attended, convolved, att_rows, conv_rows)
+
+
 def local(
     tokens,
     norm_gain,
@@ -431,13 +528,7 @@
             jnp.float32
         )
     convolved = (gate_b.astype(jnp.float32) * summed).astype(jnp.bfloat16)
-    contract = (((1,), (1,)), ((), ()))
-    share = lax.dot_general(attended, att_rows, contract, preferred_element_type=jnp.float32)
-    share = share + lax.dot_general(
-        convolved, conv_rows, contract, preferred_element_type=jnp.float32
-    )
-    rounded = share.astype(jnp.bfloat16).astype(jnp.float32)
-    mixed = lax.psum_scatter(rounded.astype(jnp.bfloat16), "tp", scatter_dimension=0, tiled=True)
+    mixed = mixed_rows(attended, convolved, att_rows, conv_rows)
     return (mixed, log_weight)
 
 

time: 164 us -> 134 us (0.82)
  the two profiles are of different devices: /device:TPU:1 before, /device:TPU:248 now
where the time goes in v3:
time: 134 us
  Pallas kernels  114 us (85%)
  local copies, waits for them, and re-layouts  8.1 us (6%)
  matrix products  6.68 us (5%)
  starting transfers between devices  2.4 us (2%)
    pallas_call x1, Pallas kernels, gathered_keys(): pl.pallas_call(keys_kernel, name='gather_keys', out_shape=(jax.ShapeDtype...  35.1 us
    pallas_call x1, Pallas kernels, attend(): pl.pallas_call(attention_kernel, name='attention', out_shape=(jax.ShapeDt...  32.4 us
    pallas_call x1, Pallas kernels, gathered_rows(): pl.pallas_call(tokens_kernel, name='gather_rows', out_shape=(jax.ShapeDty...  24.8 us
    pallas_call x1, Pallas kernels, mixed_rows(): pl.pallas_call(output_kernel, name='output', out_shape=jax.ShapeDtypeStru...  22.2 us
    unnamed x34, local copies, waits for them, and re-layouts  7.84 us
    dot_general x6, matrix products, project(): jnp.dot(normed, weight, preferred_element_type=jnp.float32)  6.68 us
  transfers between devices with their start and end apart: 1, of which 0 were waited for; matrix products, arithmetic and copies ran while one was open for 2% of the time, Pallas kernels for 50%

profile of v3, /device:TPU:248, one launch (start us, length us, event | category | flops | bytes accessed | tf_op | source)
XLA Modules:
  0.0 133.8 jit_solution(4988941884209841830)
XLA Ops:
  0.6 0.0 copy-start
  0.7 1.2 copy-done.5
  1.8 0.8 copy-done.6
  2.6 0.8 copy-done.7
  3.4 24.8 %gather_rows.1 = (bf16[256,4096]{1,0:T(8,128)(2,1)S(1)}, bf16[4096,256]{1,0:T(8,128)(2,1)S(1)}, bf16[4096,256]{1,0:T(8,128)(2,1)S(1)}) custom-call(bf16[64,4096]{1,0:T(8,128)(2,1)S(1)} %copy-done.5, bf16[64,256]{1,0:T(8,128)(2,1)S(1)} %copy-done.6, bf16[64,256]{1,0:T(8,128)(2,1)S(1)} %copy-done.7), custom_call_target="tpu_custom_call" | custom-call | tf_op jit(solution)/shard_map/gather_rows/pallas_call | solution.py:363
  28.2 0.5 fusion
  28.7 0.0 copy-done.13
  28.7 0.6 fusion.2
  29.4 0.2 copy-done.1
  29.5 0.6 copy-done.3
  30.2 0.7 fusion.6
  30.9 1.6 %copy-done.10 = bf16[4096,256]{1,0:T(8,128)(2,1)S(1)} copy-done((bf16[4096,256]{1,0:T(8,128)(2,1)S(1)}, bf16[4096,256]{1,0:T(8,128)(2,1)}, u32[]{:S(2)}) %copy-start.10) | copy-done | bytes 2097176
  32.5 0.7 fusion.5
  33.2 0.0 copy-start.12
  33.3 2.4 %collective-permute-start = (bf16[2,256]{1,0:T(2,128)(2,1)S(1)}, bf16[2,256]{1,0:T(2,128)(2,1)S(1)}, u32[]{:S(2)}, u32[]{:S(2)}) collective-permute-start(bf16[2,256]{1,0:T(2,128)(2,1)S(1)} %slice.28), channel_id=1, source_target_pairs={{0,4},{4,8},{8,12},{12,16},{16,20},{20,24},{24,28},{28,32},{32,36}... | collective-permute-start | bytes 3080 | tf_op jit(solution)/shard_map/ppermute | solution.py:17
  35.7 0.0 copy-done.11
  35.7 0.7 convolution_convert_fusion.4.value_ref
  36.4 0.0 copy-start.15
  36.5 0.7 convolution_convert_fusion.5.key_ref
  37.2 0.8 copy-done.15
  38.0 0.7 convolution_convert_fusion.3.q_ref
  38.8 35.1 %gather_keys.1 = (bf16[16384,128]{1,0:T(8,128)(2,1)S(1)}, bf16[16384,128]{1,0:T(8,128)(2,1)S(1)}) custom-call(bf16[256,128]{1,0:T(8,128)(2,1)S(1)} %convolution_convert_fusion.5.key_ref, bf16[256,128]{1,0:T(8,128)(2,1)S(1)} %convolution_convert_fusion.4.value_ref), custom_call_target="tpu_custom_call" | custom-call | tf_op jit(solution)/shard_map/gather_keys/pallas_call | solution.py:289
  73.9 0.0 copy-start.14
  73.9 32.4 %attention.1 = (bf16[256,256]{1,0:T(8,128)(2,1)S(1)}, f32[256,256]{1,0:T(8,128)S(1)}) custom-call(bf16[256,256]{1,0:T(8,128)(2,1)S(1)} %convolution_convert_fusion.3.q_ref, bf16[16384,128]{1,0:T(8,128)(2,1)S(1)} %get-tuple-element.10.k_ref, bf16[16384,128]{1,0:T(8,128)(2,1)S(1)} %get-tuple-element.11.v_ref, f32[2]{0:T(128)S(1)} %copy-done.8, ...), custom_call_target="tpu_custom_call" | custom-call | flops 12000000000 | bytes 9000000 | tf_op jit(solution)/shard_map/attention/pallas_call | solution.py:118
  106.3 0.3 slice.27
  106.6 0.1 maximum_log_fusion
  106.7 0.7 copy.14
  107.3 0.0 collective-permute-done
  107.3 3.1 %fusion.9.conv_ref = bf16[256,256]{1,0:T(8,128)(2,1)S(1)} fusion(bf16[256,4096]{1,0:T(8,128)(2,1)} %copy-done.9, bf16[4096,256]{1,0:T(8,128)(2,1)} %param.18, bf16[256,256]{1,0:T(8,128)(2,1)S(1)} %fusion.5, bf16[2,256]{1,0:T(2,128)(2,1)S(1)} %collective-permute-done, f32[256]{0:T(256)S(1)} %bitcast.16, f32[256]{0:T(256)S(1)} %bitcast.17, f32[256]{0:T(256)S(1)} %bitcast.15), kind=kOutput, calls=%fused_computation.14 | convolution fusion | flops 538050560 | bytes 4460544 | tf_op jit(solution)/shard_map/dot_general | solution.py:502
  110.4 0.4 copy-done.4
  110.8 22.2 %output.1 = bf16[64,4096]{1,0:T(8,128)(2,1)S(1)} custom-call(bf16[256,256]{1,0:T(8,128)(2,1)S(1)} %get-tuple-element.12.att_ref, bf16[256,256]{1,0:T(8,128)(2,1)S(1)} %fusion.9.conv_ref, bf16[4096,256]{1,0:T(8,128)(2,1)S(1)} %copy-done.2, bf16[4096,256]{1,0:T(8,128)(2,1)S(1)} %copy-done.4), custom_call_target="tpu_custom_call" | custom-call | tf_op jit(solution)/shard_map/output/pallas_call | solution.py:466
  133.0 0.8 copy.16
  (22 shorter events, 0.1 us)
Async XLA Ops:
  0.6 29.5 %copy-start = (bf16[4096,256]{1,0:T(8,128)(2,1)S(1)}, bf16[4096,256]{1,0:T(8,128)(2,1)}, u32[]{:S(2)}) copy-start(bf16[4096,256]{1,0:T(8,128)(2,1)} %param.19) | copy-start | bytes 6291460
  0.6 1.2 copy-start.5
  1.8 0.8 copy-start.6
  2.6 0.8 copy-start.7
  3.4 25.4 %copy-start.13 = (f32[4096]{0:T(1024)S(1)}, f32[4096]{0:T(1024)}, u32[]{:S(2)}) copy-start(f32[4096]{0:T(1024)} %param.13) | copy-start | bytes 49156
  28.2 1.3 %copy-start.1 = (bf16[4096,256]{1,0:T(8,128)(2,1)}, bf16[4096,256]{1,0:T(8,128)(2,1)S(1)}, u32[]{:S(2)}) copy-start(bf16[4096,256]{1,0:T(8,128)(2,1)S(1)} %get-tuple-element.13.att_rows) | copy-start | bytes 6291460
  28.2 1.9 %copy-start.3 = (bf16[4096,256]{1,0:T(8,128)(2,1)}, bf16[4096,256]{1,0:T(8,128)(2,1)S(1)}, u32[]{:S(2)}) copy-start(bf16[4096,256]{1,0:T(8,128)(2,1)S(1)} %get-tuple-element.14.conv_rows) | copy-start | bytes 6291460
  30.1 7.0 %copy-start.9 = (bf16[256,4096]{1,0:T(8,128)(2,1)}, bf16[256,4096]{1,0:T(8,128)(2,1)S(1)}, u32[]{:S(2)}) copy-start(bf16[256,4096]{1,0:T(8,128)(2,1)S(1)} %fusion.2) | copy-start | bytes 6291460
  30.1 2.3 %copy-start.10 = (bf16[4096,256]{1,0:T(8,128)(2,1)S(1)}, bf16[4096,256]{1,0:T(8,128)(2,1)}, u32[]{:S(2)}) copy-start(bf16[4096,256]{1,0:T(8,128)(2,1)} %param.20) | copy-start | bytes 6291460
  32.5 3.2 %copy-start.11 = (bf16[4096,128]{1,0:T(8,128)(2,1)S(1)}, bf16[4096,128]{1,0:T(8,128)(2,1)}, u32[]{:S(2)}) copy-start(bf16[4096,128]{1,0:T(8,128)(2,1)} %param.16) | copy-start | bytes 3145732
  33.2 3.2 %copy-start.12 = (bf16[4096,128]{1,0:T(8,128)(2,1)S(1)}, bf16[4096,128]{1,0:T(8,128)(2,1)}, u32[]{:S(2)}) copy-start(bf16[4096,128]{1,0:T(8,128)(2,1)} %param.15) | copy-start | bytes 3145732
  33.3 74.1 %collective-permute-start = (bf16[2,256]{1,0:T(2,128)(2,1)S(1)}, bf16[2,256]{1,0:T(2,128)(2,1)S(1)}, u32[]{:S(2)}, u32[]{:S(2)}) collective-permute-start(bf16[2,256]{1,0:T(2,128)(2,1)S(1)} %slice.28), channel_id=1, source_target_pairs={{0,4},{4,8},{8,12},{12,16},{16,20},{20,24},{24,28},{28,32},{32,36}... | collective-permute-start | bytes 3080 | tf_op jit(solution)/shard_map/ppermute | solution.py:17
  36.4 1.6 %copy-start.15 = (bf16[4096,256]{1,0:T(8,128)(2,1)S(1)}, bf16[4096,256]{1,0:T(8,128)(2,1)}, u32[]{:S(2)}) copy-start(bf16[4096,256]{1,0:T(8,128)(2,1)} %param.14) | copy-start | bytes 6291460
  38.0 35.8 %copy-start.8 = (f32[2]{0:T(128)S(1)}, f32[2]{0:T(128)}, u32[]{:S(2)}) copy-start(f32[2]{0:T(128)} %shift_ref.1) | copy-start | bytes 28
  73.9 32.8 %copy-start.14 = (f32[3,256]{1,0:T(4,128)S(1)}, f32[3,256]{1,0:T(4,128)}, u32[]{:S(2)}) copy-start(f32[3,256]{1,0:T(4,128)} %param.21) | copy-start | bytes 9220
  107.3 3.1 %copy-start.2 = (bf16[4096,256]{1,0:T(8,128)(2,1)S(1)}, bf16[4096,256]{1,0:T(8,128)(2,1)}, u32[]{:S(2)}) copy-start(bf16[4096,256]{1,0:T(8,128)(2,1)} %copy-done.1) | copy-start | bytes 6291460
  107.3 3.5 %copy-start.4 = (bf16[4096,256]{1,0:T(8,128)(2,1)S(1)}, bf16[4096,256]{1,0:T(8,128)(2,1)}, u32[]{:S(2)}) copy-start(bf16[4096,256]{1,0:T(8,128)(2,1)} %copy-done.3) | copy-start | bytes 6291460

commit v4 on v3

--- a/solution.py
+++ b/solution.py
@@ -108,7 +108,7 @@
 
     for h in range(2):
         out_ref[:, h * HEAD_DIM : (h + 1) * HEAD_DIM] = acc[heads[h], :].astype(BF16)
-        sum_ref[:, h * HEAD_DIM : (h + 1) * HEAD_DIM] = carry[heads[h], :]
+        sum_ref[h : h + 1, :] = jnp.transpose(carry[heads[h], :])[0:1, :]
 
 
 def attend(queries, key_whole, value_whole, score_shift):
@@ -120,7 +120,7 @@
         name="attention",
         out_shape=(
             jax.ShapeDtypeStruct((row_count, width), BF16),
-            jax.ShapeDtypeStruct((row_count, width), F32),
+            jax.ShapeDtypeStruct((2, row_count), F32),
         ),
         in_specs=[vmem, vmem, vmem, pl.BlockSpec(memory_space=pltpu.SMEM), vmem],
         out_specs=(vmem, vmem),
@@ -132,12 +132,12 @@
             pltpu.VMEM((2, 2 * TILE, TILE), F32),
             pltpu.VMEM((2, 2 * TILE, TILE), F32),
         ],
-        compiler_params=pltpu.CompilerParams(vmem_limit_bytes=40 * 1024 * 1024),
+        compiler_params=pltpu.CompilerParams(vmem_limit_bytes=16 * 1024 * 1024),
         cost_estimate=pl.CostEstimate(
             flops=12 * 10**9, bytes_accessed=9 * 10**6, transcendentals=25 * 10**6
         ),
     )(queries, key_whole, value_whole, score_shift, later)
-    return attended, sums[:, ::HEAD_DIM]
+    return attended, sums
 
 
 UP, DOWN, NEXT, BACK, OTHER = range(5)
@@ -263,8 +263,16 @@
 )
 
 
-def keys_kernel(key_ref, value_ref, key_out, value_out, here_sem, side_sem, send_sem, own_sem):
+PROJECT_AFTER = (8, 16, 24, 32)
+
+
+def keys_kernel(
+    key_ref, value_ref, normed_ref, wq_ref, wb_ref, wc_ref, wu_ref,
+    key_out, value_out, query_out, gate_b_out, gate_c_out, input_out,
+    here_sem, side_sem, send_sem, own_sem,
+):
     gather = Gather((key_ref, value_ref), (key_out, value_out), key_ref.shape[0], here_sem, side_sem, send_sem)
+    weights = (wq_ref, wb_ref, wc_ref, wu_ref)
     greet(gather)
     gather.begin()
     kept = [
@@ -273,7 +281,13 @@
     ]
     for copy in kept:
         copy.start()
-    for key in gather.order:
+    outs = (query_out, gate_b_out, gate_c_out, input_out)
+    for position, key in enumerate(gather.order):
+        if position in PROJECT_AFTER:
+            number = PROJECT_AFTER.index(position)
+            outs[number][...] = jnp.dot(
+                normed_ref[...], weights[number][...], preferred_element_type=F32
+            ).astype(BF16)
         gather.arrive(key)
     for half in range(2):
         for dz in range(-3, 5):
@@ -283,20 +297,24 @@
     gather.finish()
 
 
-def gathered_keys(keys, values):
+def gathered_keys(keys, values, normed, weights):
     shape = (keys.shape[0] * ZS * YS * CORES, keys.shape[1])
     vmem = pl.BlockSpec(memory_space=pltpu.VMEM)
+    projected = jax.ShapeDtypeStruct((normed.shape[0], weights[0].shape[1]), BF16)
     return pl.pallas_call(
         keys_kernel,
         name="gather_keys",
-        out_shape=(jax.ShapeDtypeStruct(shape, BF16),) * 2,
-        in_specs=[vmem] * 2,
-        out_specs=(vmem,) * 2,
-        scratch_shapes=[*GATHER_SEMS, pltpu.SemaphoreType.DMA((2,))],
+        out_shape=(jax.ShapeDtypeStruct(shape, BF16),) * 2 + (projected,) * 4,
+        in_specs=[vmem] * 7,
+        out_specs=(vmem,) * 6,
+        scratch_shapes=[
+            *GATHER_SEMS,
+            pltpu.SemaphoreType.DMA((2,)),
+        ],
         compiler_params=pltpu.CompilerParams(
             collective_id=1, has_side_effects=True, vmem_limit_bytes=24 * 1024 * 1024
         ),
-    )(keys, values)
+    )(keys, values, normed, *weights)
 
 
 def tokens_kernel(
@@ -368,7 +386,7 @@
             jax.ShapeDtypeStruct((w_out_att.shape[0] * many, w_out_att.shape[1]), BF16),
             jax.ShapeDtypeStruct((w_out_conv.shape[0] * many, w_out_conv.shape[1]), BF16),
         ),
-        in_specs=[vmem] * 3,
+        in_specs=[pl.BlockSpec(memory_space=pltpu.HBM)] * 3,
         out_specs=(vmem,) * 3,
         scratch_shapes=[
             *GATHER_SEMS,
@@ -493,34 +511,20 @@
     w_out_att,
     w_out_conv,
 ):
-    weights = (w_query, w_key, w_value, w_conv_b, w_conv_c, w_conv_u)
-
-    def project(rows_in):
-        normed = normalize(rows_in, norm_gain)
-        return jnp.concatenate(
-            [
-                jnp.dot(normed, weight, preferred_element_type=jnp.float32).astype(jnp.bfloat16)
-                for weight in weights
-            ],
-            axis=1,
-        )
-
     rows, att_rows, conv_rows = gathered_rows(tokens, w_out_att, w_out_conv)
-    projected = project(rows)
-    widths = [weight.shape[1] for weight in weights]
-    edges = [0]
-    for width in widths:
-        edges.append(edges[-1] + width)
-    queries, keys, values, gate_b, gate_c, inputs_u = [
-        projected[:, edges[pos] : edges[pos + 1]] for pos in range(6)
+    normed = normalize(rows, norm_gain)
+    keys, values = [
+        jnp.dot(normed, weight, preferred_element_type=jnp.float32).astype(jnp.bfloat16)
+        for weight in (w_key, w_value)
     ]
-    tok_count = projected.shape[0]
-    conv_local = gate_b.shape[1]
+    key_whole, value_whole, queries, gate_b, gate_c, inputs_u = gathered_keys(
+        keys, values, normed, (w_query, w_conv_b, w_conv_c, w_conv_u)
+    )
+    tok_count, conv_local = gate_b.shape
     products = (gate_c.astype(jnp.float32) * inputs_u.astype(jnp.float32)).astype(jnp.bfloat16)
     previous = shifted(products[tok_count - (CONV_K - 1) :], "sp", 1)
-    key_whole, value_whole = gathered_keys(keys, values)
     attended, sums_all = attend(queries, key_whole, value_whole, score_shift)
-    log_weight = jnp.log(jnp.maximum(-jnp.expm1(-sums_all), 0.05))
+    log_weight = jnp.log(jnp.maximum(-jnp.expm1(-sums_all), 0.05)).T
     extended = jnp.concatenate([previous, products], axis=0)
     summed = jnp.zeros((tok_count, conv_local), jnp.float32)
     for tap in range(CONV_K):

time: 134 us -> 124 us (0.925)
  matrix products: 6.68 us -> 1.41 us
  local copies, waits for them, and re-layouts: 8.1 us -> 5.31 us
  Pallas kernels: 114 us -> 112 us
    dot_general x6 -> x2, matrix products: 6.68 us -> 1.41 us  [local(): jnp.dot(normed, weight, preferred_element_type=jnp.float32)]
    unnamed x34 -> x25, local copies, waits for them, and re-layouts: 7.84 us -> 5.3 us
    pallas_call x1, Pallas kernels: 35.1 us -> 33.6 us  [gathered_keys(): pl.pallas_call(keys_kernel, name='gather_keys', out_shape=(jax.ShapeDtype...]
  transfers between devices with their start and end apart: 1 -> 1, of which waited for: 0 -> 0; matrix products, arithmetic and copies ran while one was open for 2% -> 1% of each run, Pallas kernels for 50% -> 26%
where the time goes in v4:
time: 124 us
  Pallas kernels  112 us (90%)
  local copies, waits for them, and re-layouts  5.31 us (4%)
  starting transfers between devices  2.27 us (2%)
  other arithmetic  1.92 us (2%)
  matrix products  1.41 us (1%)
    pallas_call x1, Pallas kernels, gathered_keys(): pl.pallas_call(keys_kernel, name='gather_keys', out_shape=(jax.ShapeDtype...  33.6 us
    pallas_call x1, Pallas kernels, attend(): pl.pallas_call(attention_kernel, name='attention', out_shape=(jax.ShapeDt...  32.6 us
    pallas_call x1, Pallas kernels, gathered_rows(): pl.pallas_call(tokens_kernel, name='gather_rows', out_shape=(jax.ShapeDty...  24.8 us
    pallas_call x1, Pallas kernels, mixed_rows(): pl.pallas_call(output_kernel, name='output', out_shape=jax.ShapeDtypeStru...  21.4 us
    unnamed x25, local copies, waits for them, and re-layouts  5.3 us
  transfers between devices with their start and end apart: 1, of which 0 were waited for; matrix products, arithmetic and copies ran while one was open for 1% of the time, Pallas kernels for 26%

profile of v4, /device:TPU:248, one launch (start us, length us, event | category | flops | bytes accessed | tf_op | source)
XLA Modules:
  0.0 124.2 jit_solution(9080162772489570625)
XLA Ops:
  0.6 0.0 copy-start
  0.6 0.0 copy-start.5
  0.7 1.1 copy-done.5
  1.8 0.8 copy-done.6
  2.5 0.8 copy-done.7
  3.3 24.8 %gather_rows.1 = (bf16[256,4096]{1,0:T(8,128)(2,1)S(1)}, bf16[4096,256]{1,0:T(8,128)(2,1)S(1)}, bf16[4096,256]{1,0:T(8,128)(2,1)S(1)}) custom-call(bf16[64,4096]{1,0:T(8,128)(2,1)S(1)} %copy-done.5, bf16[64,256]{1,0:T(8,128)(2,1)S(1)} %copy-done.6, bf16[64,256]{1,0:T(8,128)(2,1)S(1)} %copy-done.7), custom_call_target="tpu_custom_call" | custom-call | tf_op jit(solution)/shard_map/gather_rows/pallas_call | solution.py:381
  28.1 0.5 fusion
  28.6 0.0 copy-done.10
  28.6 0.0 copy-start.9
  28.6 0.0 copy-start.4
  28.7 0.6 fusion.2.normed_ref
  29.3 0.0 copy-done
  29.3 0.0 copy-start.2
  29.3 0.0 copy-start.3
  29.3 0.7 convolution_convert_fusion.value_ref
  30.0 0.0 copy-done.9
  30.0 0.0 copy-start.1
  30.1 0.7 convolution_convert_fusion.1.key_ref
  30.8 0.0 copy-done.4
  30.8 0.6 copy-done.2
  31.3 0.6 copy-done.3
  32.0 0.6 copy-done.1
  32.6 33.6 %gather_keys.1 = (bf16[16384,128]{1,0:T(8,128)(2,1)S(1)}, bf16[16384,128]{1,0:T(8,128)(2,1)S(1)}, bf16[256,256]{1,0:T(8,128)(2,1)S(1)}, bf16[256,256]{1,0:T(8,12...) custom-call(bf16[256,128]{1,0:T(8,128)(2,1)S(1)} %convolution_convert_fusion.1.key_ref, ...), custom_call_target="tpu_custom_call" | custom-call | tf_op jit(solution)/shard_map/gather_keys/pallas_call | solution.py:304
  66.3 2.3 %collective-permute-start = (bf16[2,256]{1,0:T(2,128)(2,1)S(1)}, bf16[2,256]{1,0:T(2,128)(2,1)S(1)}, u32[]{:S(2)}, u32[]{:S(2)}) collective-permute-start(bf16[2,256]{1,0:T(2,128)(2,1)S(1)} %slice.24), channel_id=1, source_target_pairs={{0,4},{4,8},{8,12},{12,16},{16,20},{20,24},{24,28},{28,32},{32,36}... | collective-permute-start | bytes 3080 | tf_op jit(solution)/shard_map/ppermute | solution.py:17
  68.6 0.0 copy-done.11
  68.6 0.0 copy-done.8
  68.6 32.6 %attention.1 = (bf16[256,256]{1,0:T(8,128)(2,1)S(1)}, f32[2,256]{1,0:T(2,128)S(1)}) custom-call(bf16[256,256]{1,0:T(8,128)(2,1)S(1)} %get-tuple-element.14.q_ref, bf16[16384,128]{1,0:T(8,128)(2,1)S(1)} %get-tuple-element.15.k_ref, bf16[16384,128]{1,0:T(8,128)(2,1)S(1)} %get-tuple-element.16.v_ref, f32[2]{0:T(128)S(1)} %copy-done.8, ...), custom_call_target="tpu_custom_call" | custom-call | flops 12000000000 | bytes 9000000 | tf_op jit(solution)/shard_map/attention/pallas_call | solution.py:118
  101.3 0.6 log_bitcast_fusion
  101.9 0.0 collective-permute-done
  101.9 0.1 multiply_convert_fusion.conv_ref
  102.0 21.4 %output.1 = bf16[64,4096]{1,0:T(8,128)(2,1)S(1)} custom-call(bf16[256,256]{1,0:T(8,128)(2,1)S(1)} %get-tuple-element.17.att_ref, bf16[256,256]{1,0:T(8,128)(2,1)S(1)} %multiply_convert_fusion.conv_ref, bf16[4096,256]{1,0:T(8,128)(2,1)S(1)} %get-tuple-element.21.att_rows, bf16[4096,256]{1,0:T(8,128)(2,1)S(1)} %get-tuple-element.22.conv_rows), custom_call_target="tpu_custom_call" | custom-call | tf_op jit(solution)/shard_map/output/pallas_call | solution.py:484
  123.4 0.8 copy.15
  (10 shorter events, 0.1 us)
Async XLA Ops:
  0.6 28.7 %copy-start = (bf16[4096,128]{1,0:T(8,128)(2,1)S(1)}, bf16[4096,128]{1,0:T(8,128)(2,1)}, u32[]{:S(2)}) copy-start(bf16[4096,128]{1,0:T(8,128)(2,1)} %param.16) | copy-start | bytes 3145732
  0.6 1.1 copy-start.5
  1.8 0.8 copy-start.6
  2.5 0.8 copy-start.7
  3.3 25.3 %copy-start.10 = (f32[4096]{0:T(1024)S(1)}, f32[4096]{0:T(1024)}, u32[]{:S(2)}) copy-start(f32[4096]{0:T(1024)} %param.13) | copy-start | bytes 49156
  28.6 1.4 %copy-start.9 = (bf16[4096,128]{1,0:T(8,128)(2,1)S(1)}, bf16[4096,128]{1,0:T(8,128)(2,1)}, u32[]{:S(2)}) copy-start(bf16[4096,128]{1,0:T(8,128)(2,1)} %param.15) | copy-start | bytes 3145732
  28.6 2.1 %copy-start.4 = (bf16[4096,256]{1,0:T(8,128)(2,1)S(1)}, bf16[4096,256]{1,0:T(8,128)(2,1)}, u32[]{:S(2)}) copy-start(bf16[4096,256]{1,0:T(8,128)(2,1)} %wu_ref.1) | copy-start | bytes 6291460
  29.3 2.0 %copy-start.2 = (bf16[4096,256]{1,0:T(8,128)(2,1)S(1)}, bf16[4096,256]{1,0:T(8,128)(2,1)}, u32[]{:S(2)}) copy-start(bf16[4096,256]{1,0:T(8,128)(2,1)} %wb_ref.1) | copy-start | bytes 6291460
  29.3 2.7 %copy-start.3 = (bf16[4096,256]{1,0:T(8,128)(2,1)S(1)}, bf16[4096,256]{1,0:T(8,128)(2,1)}, u32[]{:S(2)}) copy-start(bf16[4096,256]{1,0:T(8,128)(2,1)} %wc_ref.1) | copy-start | bytes 6291460
  30.0 2.6 %copy-start.1 = (bf16[4096,256]{1,0:T(8,128)(2,1)S(1)}, bf16[4096,256]{1,0:T(8,128)(2,1)}, u32[]{:S(2)}) copy-start(bf16[4096,256]{1,0:T(8,128)(2,1)} %wq_ref.1) | copy-start | bytes 6291460
  32.6 36.0 %copy-start.11 = (f32[3,256]{1,0:T(4,128)S(1)}, f32[3,256]{1,0:T(4,128)}, u32[]{:S(2)}) copy-start(f32[3,256]{1,0:T(4,128)} %param.21) | copy-start | bytes 9220
  32.6 36.0 %copy-start.8 = (f32[2]{0:T(128)S(1)}, f32[2]{0:T(128)}, u32[]{:S(2)}) copy-start(f32[2]{0:T(128)} %shift_ref.1) | copy-start | bytes 28
  66.3 35.6 %collective-permute-start = (bf16[2,256]{1,0:T(2,128)(2,1)S(1)}, bf16[2,256]{1,0:T(2,128)(2,1)S(1)}, u32[]{:S(2)}, u32[]{:S(2)}) collective-permute-start(bf16[2,256]{1,0:T(2,128)(2,1)S(1)} %slice.24), channel_id=1, source_target_pairs={{0,4},{4,8},{8,12},{12,16},{16,20},{20,24},{24,28},{28,32},{32,36}... | collective-permute-start | bytes 3080 | tf_op jit(solution)/shard_map/ppermute | solution.py:17

commit v5 on v4

--- a/solution.py
+++ b/solution.py
@@ -263,7 +263,7 @@
 )
 
 
-PROJECT_AFTER = (8, 16, 24, 32)
+PROJECT_AFTER = (0, 0, 0, 0)
 
 
 def keys_kernel(
@@ -283,8 +283,7 @@
         copy.start()
     outs = (query_out, gate_b_out, gate_c_out, input_out)
     for position, key in enumerate(gather.order):
-        if position in PROJECT_AFTER:
-            number = PROJECT_AFTER.index(position)
+        for number in [n for n in range(4) if PROJECT_AFTER[n] == position]:
             outs[number][...] = jnp.dot(
                 normed_ref[...], weights[number][...], preferred_element_type=F32
             ).astype(BF16)

time: 124 us -> 124 us (level)
  no operation moved by 1% of the time
where the time goes in v5:
time: 124 us
  Pallas kernels  112 us (90%)
  local copies, waits for them, and re-layouts  5.31 us (4%)
  starting transfers between devices  2.27 us (2%)
  other arithmetic  1.92 us (2%)
  matrix products  1.41 us (1%)
    pallas_call x1, Pallas kernels, gathered_keys(): pl.pallas_call(keys_kernel, name='gather_keys', out_shape=(jax.ShapeDtype...  33.6 us
    pallas_call x1, Pallas kernels, attend(): pl.pallas_call(attention_kernel, name='attention', out_shape=(jax.ShapeDt...  32.5 us
    pallas_call x1, Pallas kernels, gathered_rows(): pl.pallas_call(tokens_kernel, name='gather_rows', out_shape=(jax.ShapeDty...  24.8 us
    pallas_call x1, Pallas kernels, mixed_rows(): pl.pallas_call(output_kernel, name='output', out_shape=jax.ShapeDtypeStru...  21.3 us
    unnamed x25, local copies, waits for them, and re-layouts  5.3 us
  transfers between devices with their start and end apart: 1, of which 0 were waited for; matrix products, arithmetic and copies ran while one was open for 1% of the time, Pallas kernels for 26%

profile of v5, /device:TPU:248, one launch (start us, length us, event | category | flops | bytes accessed | tf_op | source)
XLA Modules:
  0.0 124.0 jit_solution(6052320435161082615)
XLA Ops:
  0.6 0.0 copy-start
  0.6 0.0 copy-start.5
  0.7 1.1 copy-done.5
  1.8 0.8 copy-done.6
  2.5 0.8 copy-done.7
  3.3 24.8 %gather_rows.1 = (bf16[256,4096]{1,0:T(8,128)(2,1)S(1)}, bf16[4096,256]{1,0:T(8,128)(2,1)S(1)}, bf16[4096,256]{1,0:T(8,128)(2,1)S(1)}) custom-call(bf16[64,4096]{1,0:T(8,128)(2,1)S(1)} %copy-done.5, bf16[64,256]{1,0:T(8,128)(2,1)S(1)} %copy-done.6, bf16[64,256]{1,0:T(8,128)(2,1)S(1)} %copy-done.7), custom_call_target="tpu_custom_call" | custom-call | tf_op jit(solution)/shard_map/gather_rows/pallas_call | solution.py:380
  28.1 0.5 fusion
  28.6 0.0 copy-done.10
  28.6 0.0 copy-start.9
  28.6 0.0 copy-start.4
  28.7 0.6 fusion.2.normed_ref
  29.3 0.0 copy-done
  29.3 0.0 copy-start.2
  29.3 0.0 copy-start.3
  29.3 0.7 convolution_convert_fusion.value_ref
  30.0 0.0 copy-done.9
  30.0 0.0 copy-start.1
  30.1 0.7 convolution_convert_fusion.1.key_ref
  30.8 0.0 copy-done.4
  30.8 0.6 copy-done.2
  31.3 0.6 copy-done.3
  32.0 0.6 copy-done.1
  32.6 33.6 %gather_keys.1 = (bf16[16384,128]{1,0:T(8,128)(2,1)S(1)}, bf16[16384,128]{1,0:T(8,128)(2,1)S(1)}, bf16[256,256]{1,0:T(8,128)(2,1)S(1)}, bf16[256,256]{1,0:T(8,12...) custom-call(bf16[256,128]{1,0:T(8,128)(2,1)S(1)} %convolution_convert_fusion.1.key_ref, ...), custom_call_target="tpu_custom_call" | custom-call | tf_op jit(solution)/shard_map/gather_keys/pallas_call | solution.py:303
  66.3 2.3 %collective-permute-start = (bf16[2,256]{1,0:T(2,128)(2,1)S(1)}, bf16[2,256]{1,0:T(2,128)(2,1)S(1)}, u32[]{:S(2)}, u32[]{:S(2)}) collective-permute-start(bf16[2,256]{1,0:T(2,128)(2,1)S(1)} %slice.24), channel_id=1, source_target_pairs={{0,4},{4,8},{8,12},{12,16},{16,20},{20,24},{24,28},{28,32},{32,36}... | collective-permute-start | bytes 3080 | tf_op jit(solution)/shard_map/ppermute | solution.py:17
  68.6 0.0 copy-done.11
  68.6 0.0 copy-done.8
  68.6 32.5 %attention.1 = (bf16[256,256]{1,0:T(8,128)(2,1)S(1)}, f32[2,256]{1,0:T(2,128)S(1)}) custom-call(bf16[256,256]{1,0:T(8,128)(2,1)S(1)} %get-tuple-element.14.q_ref, bf16[16384,128]{1,0:T(8,128)(2,1)S(1)} %get-tuple-element.15.k_ref, bf16[16384,128]{1,0:T(8,128)(2,1)S(1)} %get-tuple-element.16.v_ref, f32[2]{0:T(128)S(1)} %copy-done.8, ...), custom_call_target="tpu_custom_call" | custom-call | flops 12000000000 | bytes 9000000 | tf_op jit(solution)/shard_map/attention/pallas_call | solution.py:118
  101.1 0.6 log_bitcast_fusion
  101.7 0.0 collective-permute-done
  101.7 0.1 multiply_convert_fusion.conv_ref
  101.8 21.3 %output.1 = bf16[64,4096]{1,0:T(8,128)(2,1)S(1)} custom-call(bf16[256,256]{1,0:T(8,128)(2,1)S(1)} %get-tuple-element.17.att_ref, bf16[256,256]{1,0:T(8,128)(2,1)S(1)} %multiply_convert_fusion.conv_ref, bf16[4096,256]{1,0:T(8,128)(2,1)S(1)} %get-tuple-element.21.att_rows, bf16[4096,256]{1,0:T(8,128)(2,1)S(1)} %get-tuple-element.22.conv_rows), custom_call_target="tpu_custom_call" | custom-call | tf_op jit(solution)/shard_map/output/pallas_call | solution.py:483
  123.2 0.8 copy.15
  (10 shorter events, 0.1 us)
Async XLA Ops:
  0.6 28.7 %copy-start = (bf16[4096,128]{1,0:T(8,128)(2,1)S(1)}, bf16[4096,128]{1,0:T(8,128)(2,1)}, u32[]{:S(2)}) copy-start(bf16[4096,128]{1,0:T(8,128)(2,1)} %param.16) | copy-start | bytes 3145732
  0.6 1.1 copy-start.5
  1.8 0.8 copy-start.6
  2.5 0.8 copy-start.7
  3.3 25.3 %copy-start.10 = (f32[4096]{0:T(1024)S(1)}, f32[4096]{0:T(1024)}, u32[]{:S(2)}) copy-start(f32[4096]{0:T(1024)} %param.13) | copy-start | bytes 49156
  28.6 1.4 %copy-start.9 = (bf16[4096,128]{1,0:T(8,128)(2,1)S(1)}, bf16[4096,128]{1,0:T(8,128)(2,1)}, u32[]{:S(2)}) copy-start(bf16[4096,128]{1,0:T(8,128)(2,1)} %param.15) | copy-start | bytes 3145732
  28.6 2.1 %copy-start.4 = (bf16[4096,256]{1,0:T(8,128)(2,1)S(1)}, bf16[4096,256]{1,0:T(8,128)(2,1)}, u32[]{:S(2)}) copy-start(bf16[4096,256]{1,0:T(8,128)(2,1)} %wu_ref.1) | copy-start | bytes 6291460
  29.3 2.0 %copy-start.2 = (bf16[4096,256]{1,0:T(8,128)(2,1)S(1)}, bf16[4096,256]{1,0:T(8,128)(2,1)}, u32[]{:S(2)}) copy-start(bf16[4096,256]{1,0:T(8,128)(2,1)} %wb_ref.1) | copy-start | bytes 6291460
  29.3 2.7 %copy-start.3 = (bf16[4096,256]{1,0:T(8,128)(2,1)S(1)}, bf16[4096,256]{1,0:T(8,128)(2,1)}, u32[]{:S(2)}) copy-start(bf16[4096,256]{1,0:T(8,128)(2,1)} %wc_ref.1) | copy-start | bytes 6291460
  30.0 2.6 %copy-start.1 = (bf16[4096,256]{1,0:T(8,128)(2,1)S(1)}, bf16[4096,256]{1,0:T(8,128)(2,1)}, u32[]{:S(2)}) copy-start(bf16[4096,256]{1,0:T(8,128)(2,1)} %wq_ref.1) | copy-start | bytes 6291460
  32.6 36.0 %copy-start.11 = (f32[3,256]{1,0:T(4,128)S(1)}, f32[3,256]{1,0:T(4,128)}, u32[]{:S(2)}) copy-start(f32[3,256]{1,0:T(4,128)} %param.21) | copy-start | bytes 9220
  32.6 36.0 %copy-start.8 = (f32[2]{0:T(128)S(1)}, f32[2]{0:T(128)}, u32[]{:S(2)}) copy-start(f32[2]{0:T(128)} %shift_ref.1) | copy-start | bytes 28
  66.3 35.4 %collective-permute-start = (bf16[2,256]{1,0:T(2,128)(2,1)S(1)}, bf16[2,256]{1,0:T(2,128)(2,1)S(1)}, u32[]{:S(2)}, u32[]{:S(2)}) collective-permute-start(bf16[2,256]{1,0:T(2,128)(2,1)S(1)} %slice.24), channel_id=1, source_target_pairs={{0,4},{4,8},{8,12},{12,16},{16,20},{20,24},{24,28},{28,32},{32,36}... | collective-permute-start | bytes 3080 | tf_op jit(solution)/shard_map/ppermute | solution.py:17
